TPU v7x, 256 devices: a whole 4x4x8 slice. The times are simulated.
256 devices in a mesh: ep: 16 (over y, x), tp: 16 (over z, core).
Axes of the slice: x: 4, y: 4, z: 8, core: 2. Of those that a mesh axis runs over, the one named last changes fastest.
Arguments:
- tokens: bfloat16 [256, 4096], P('ep'), may hold values from -6 to 6
- query_weight: bfloat16 [4096, 4096], P('ep', 'tp'), may hold values from -0.09375 to 0.09375
- key_weight: bfloat16 [4096, 2048], P('ep', 'tp'), may hold values from -0.15625 to 0.15625
- value_weight: bfloat16 [4096, 2048], P('ep', 'tp'), may hold values from -0.09375 to 0.09375
- out_weight: bfloat16 [4096, 4096], P('tp', 'ep'), may hold values from -0.09375 to 0.09375
- head_lambda: float32 [32], P('tp'), may hold values from 0.3 to 0.8
- head_gain: float32 [128], replicated, may hold values from 0.1 to 1.9
- key_cache: bfloat16 [256, 1024, 16, 128], P('ep', None, 'tp'), may hold values from -1000 to 1000
- value_cache: bfloat16 [256, 1024, 16, 128], P('ep', None, 'tp'), may hold values from -6 to 6
- lengths: int32 [256], P('ep'), may hold values from 128 to 1024, as said below
- first_gain: float32 [4096], replicated, may hold values from 0.3 to 3
- second_gain: float32 [4096], P('tp'), may hold values from 0.1 to 1.9
- expert_ids: int32 [256, 2], P('ep'), may hold values from 0 to 15, all different within a row; in each aligned block of 16 rows (0 to 15, 16 to 31, ...) at most 4 rows name the same one
- route_weights: float32 [256, 2], P('ep'), may hold values from 0.1 to 1
- expert_gate: bfloat16 [16, 4096, 2048], P('ep', 'tp'), may hold values from -0.09375 to 0.09375
- expert_up: bfloat16 [16, 4096, 2048], P('ep', 'tp'), may hold values from -0.09375 to 0.09375
- expert_down: bfloat16 [16, 2048, 4096], P('ep', None, 'tp'), may hold values from -0.125 to 0.125
- dense_gate: bfloat16 [4096, 2048], P('tp', 'ep'), may hold values from -0.09375 to 0.09375
- dense_up: bfloat16 [4096, 2048], P('tp', 'ep'), may hold values from -0.09375 to 0.09375
- dense_down: bfloat16 [2048, 4096], P('ep', 'tp'), may hold values from -0.25 to 0.25
- dense_mix: bfloat16 [4096], replicated, may hold values from -0.09375 to 0.09375
Outputs:
- layer_out: bfloat16 [256, 4096], P('ep', 'tp')
Inputs may be any that keep to these rules, and one draw needn't show every extreme that they name: `lengths`: positions below a sequence's length hold its cache; the new token stands at that position. Some sequence has length 1024 in every draw. `expert_ids`: each row names 2 different experts. Among the rows of one device's 16 sequences (aligned blocks) no expert is named more than 4 times, and in every draw some expert is named exactly 4 times in some block.
All inputs are finite; a program needn't handle non-finite values.
Results may differ from a plain program's by a relative error of at most 0.04.
Values may be sent and summed in bfloat16 or wider, within the bound.
A program may use at most 64 MiB of HBM per device.

v0:
```python
import jax
import jax.numpy as jnp
from jax import lax
from jax.sharding import PartitionSpec as P

SUB = 64
VD = 128
EXPERTS = 16
TOPK = 2
CACHE = 1024
CAP = 4


theta_base = 500000.0
score_scale = 0.125
head_scale = 0.8
residual_scale = 2.0**0.5
layer_epsilon = 1e-05
head_epsilon = 1e-06


def in_blocks(shard, dim, peers):
    shape = shard.shape
    tiles = shard.reshape(*shape[:dim], peers, shape[dim] // peers, *shape[dim + 1 :])
    return jnp.moveaxis(tiles, dim, 0)


def sent_and_summed(shard, axis, dim):
    tiles = in_blocks(shard, dim, lax.axis_size(axis))
    arrived = lax.all_to_all(tiles, axis, split_axis=0, concat_axis=0, tiled=True)
    return arrived.astype(jnp.float32).sum(axis=0)


def sent_to_all(shard, axis):
    copies = jnp.broadcast_to(shard, (lax.axis_size(axis), *shard.shape))
    return lax.all_to_all(copies, axis, split_axis=0, concat_axis=0, tiled=True)


def joined_along(tiles, dim):
    shape = list(tiles.shape[1:])
    shape[dim] *= tiles.shape[0]
    return jnp.moveaxis(tiles, 0, dim).reshape(shape)


def gathered_copies(shard, axis, dim):
    tiles = sent_to_all(shard, axis)
    return joined_along(tiles, dim)


def over_pieces(shard, axis):
    return lax.all_gather(shard, axis).astype(jnp.float32).sum(0)


def packed_total(arrays, axis):
    ends = [0]
    for a in arrays:
        ends.append(ends[-1] + a.size)
    so_far = lax.psum(jnp.concatenate([a.ravel() for a in arrays]), axis)
    return tuple((so_far[b:e].reshape(a.shape) for a, b, e in zip(arrays, ends, ends[1:])))


def over_copies(shard, axis):
    everything = sent_to_all(shard, axis)
    return jnp.sum(everything, axis=0)


def together(arrays, axis):
    ends = [0]
    for a in arrays:
        ends.append(ends[-1] + a.size)
    so_far = over_copies(jnp.concatenate([a.ravel() for a in arrays]), axis)
    return tuple((so_far[b:e].reshape(a.shape) for a, b, e in zip(arrays, ends, ends[1:])))


def rotate(vector, cosine, sine_table):
    middle = vector.shape[-1] // 2
    lower = vector[..., :middle]
    upper = vector[..., middle:]
    return jnp.concatenate(
        [lower * cosine - upper * sine_table, upper * cosine + lower * sine_table], axis=-1
    )


def widened(array):
    return lax.optimization_barrier(array.astype(jnp.bfloat16)).astype(jnp.float32)


def attend(query_sum, key_sum, value_sum, head_lambda, head_gain, key_cache, value_cache, lengths):
    seq_count = key_cache.shape[0]
    kv_local = key_cache.shape[2]
    group_size = query_sum.shape[1] // (kv_local * 2 * SUB)
    frequency = theta_base ** (-(jnp.arange(SUB // 2, dtype=jnp.float32) * (2.0 / SUB)))
    angles = lengths.astype(jnp.float32)[:, None] * frequency[None, :]
    cosine = jnp.cos(angles)
    sine_table = jnp.sin(angles)
    query_half = widened(query_sum).reshape(seq_count, kv_local, group_size, 2, SUB)
    query_rot = rotate(
        query_half, cosine[:, None, None, None, :], sine_table[:, None, None, None, :]
    )
    query_rot = query_rot.astype(jnp.bfloat16)
    key_half = widened(key_sum).reshape(seq_count, kv_local, 2, SUB)
    key_rot = rotate(key_half, cosine[:, None, None, :], sine_table[:, None, None, :]).astype(
        jnp.bfloat16
    )
    value_new = widened(value_sum).reshape(seq_count, kv_local, 1, VD)
    cached_keys = key_cache.reshape(seq_count, CACHE, kv_local, 2, SUB)
    scores = jnp.einsum(
        "skgcd,sjkcd->skgcj", query_rot, cached_keys, preferred_element_type=jnp.float32
    )
    scores = scores * score_scale
    valid = jnp.arange(CACHE, dtype=jnp.int32)[None, :] < lengths[:, None]
    scores = jnp.where(valid[:, None, None, None, :], scores, -jnp.inf)
    fresh_score = jnp.einsum(
        "skgcd,skcd->skgc", query_rot, key_rot, preferred_element_type=jnp.float32
    )
    fresh_score = fresh_score * score_scale
    highest = jnp.maximum(jnp.max(scores, axis=-1), fresh_score)
    cached_exp = jnp.exp(scores - highest[..., None])
    fresh_exp = jnp.exp(fresh_score - highest)
    denominator = jnp.sum(cached_exp, axis=-1) + fresh_exp
    cached_prob = cached_exp / denominator[..., None]
    fresh_prob = fresh_exp / denominator
    lambdas = head_lambda.reshape(kv_local, group_size)
    mixed_map = (
        cached_prob[:, :, :, 0] - lambdas[None, :, :, None] * cached_prob[:, :, :, 1]
    ).astype(jnp.bfloat16)
    mixed_new = widened(fresh_prob[..., 0] - lambdas[None] * fresh_prob[..., 1])
    head_out = jnp.einsum(
        "skgj,sjke->skge", mixed_map, value_cache, preferred_element_type=jnp.float32
    )
    head_out = head_out + mixed_new[..., None] * value_new
    square_mean = jnp.mean(head_out * head_out, axis=-1, keepdims=True)
    normed = head_out * lax.rsqrt(square_mean + head_epsilon) * head_gain * head_scale
    return normed.astype(jnp.bfloat16).reshape(seq_count, kv_local * group_size * VD)


def on_device(
    tokens,
    query_weight,
    key_weight,
    value_weight,
    out_weight,
    head_lambda,
    head_gain,
    key_cache,
    value_cache,
    lengths,
    first_gain,
    second_gain,
    expert_ids,
    route_weights,
    expert_gate,
    expert_up,
    expert_down,
    dense_gate,
    dense_up,
    dense_down,
    dense_mix,
):
    seq_count = tokens.shape[0]
    model_width = tokens.shape[1]
    ep_count = lax.axis_size("ep")
    tp_count = lax.axis_size("tp")
    query_cols = query_weight.shape[1]
    key_cols = key_weight.shape[1]
    columns = lax.all_to_all(tokens, "ep", split_axis=1, concat_axis=0, tiled=True)
    summed = sent_and_summed(
        jnp.concatenate(
            [
                jnp.dot(columns, query_weight, preferred_element_type=jnp.float32),
                jnp.dot(columns, key_weight, preferred_element_type=jnp.float32),
                jnp.dot(columns, value_weight, preferred_element_type=jnp.float32),
            ],
            axis=1,
        ).astype(jnp.bfloat16),
        "ep",
        0,
    )
    query_sum = summed[:, :query_cols]
    key_sum = summed[:, query_cols : query_cols + key_cols]
    value_sum = summed[:, query_cols + key_cols :]
    normed = attend(
        query_sum, key_sum, value_sum, head_lambda, head_gain, key_cache, value_cache, lengths
    )
    all_heads = gathered_copies(normed, "ep", 0)
    column_part = jnp.dot(all_heads, out_weight, preferred_element_type=jnp.float32)
    column_part = over_pieces(column_part.astype(jnp.bfloat16), "tp").astype(jnp.float32)
    attention = lax.all_to_all(
        column_part.astype(jnp.bfloat16), "ep", split_axis=0, concat_axis=1, tiled=True
    )
    residual_in = residual_scale * tokens.astype(jnp.float32) + widened(attention)
    average = jnp.mean(residual_in, axis=-1, keepdims=True)
    centered = residual_in - average
    variance = jnp.mean(centered * centered, axis=-1, keepdims=True)
    hidden_in = (centered * lax.rsqrt(variance + layer_epsilon) * first_gain).astype(jnp.bfloat16)
    slice_width = model_width // tp_count
    own_cols = lax.dynamic_slice_in_dim(
        hidden_in, lax.axis_index("tp") * slice_width, slice_width, 1
    )
    flat_ids = expert_ids.reshape(-1)
    hit_table = (flat_ids[:, None] == jnp.arange(EXPERTS, dtype=jnp.int32)[None, :]).astype(
        jnp.int32
    )
    earlier = jnp.cumsum(hit_table, axis=0) - hit_table
    slot_index = jnp.sum(earlier * hit_table, axis=1)
    target = flat_ids * CAP + slot_index
    placed = jnp.arange(EXPERTS * CAP, dtype=jnp.int32)[:, None] == target[None, :]
    routed_rows = jnp.repeat(own_cols, TOPK, axis=0)
    packed = jnp.dot(placed.astype(jnp.bfloat16), routed_rows, preferred_element_type=jnp.float32)
    packed = packed.astype(jnp.bfloat16).reshape(ep_count, EXPERTS // ep_count, CAP, slice_width)
    arrived = lax.all_to_all(packed, "ep", split_axis=0, concat_axis=2, tiled=True)[0]
    expert_pre_gate = jnp.einsum(
        "erd,edf->erf", arrived, expert_gate, preferred_element_type=jnp.float32
    )
    expert_pre_up = jnp.einsum(
        "erd,edf->erf", arrived, expert_up, preferred_element_type=jnp.float32
    )
    all_rows = gathered_copies(own_cols, "ep", 0)
    dense_pre_gate = jnp.dot(all_rows, dense_gate, preferred_element_type=jnp.float32)
    dense_pre_up = jnp.dot(all_rows, dense_up, preferred_element_type=jnp.float32)
    expert_pre_gate, expert_pre_up, dense_pre_gate, dense_pre_up = tuple(
        (
            part.astype(jnp.float32)
            for part in packed_total(
                (
                    expert_pre_gate.astype(jnp.bfloat16),
                    expert_pre_up.astype(jnp.bfloat16),
                    dense_pre_gate.astype(jnp.bfloat16),
                    dense_pre_up.astype(jnp.bfloat16),
                ),
                "tp",
            )
        )
    )
    expert_hidden = (jax.nn.silu(expert_pre_gate) * expert_pre_up).astype(jnp.bfloat16)
    expert_result = jnp.einsum(
        "erf,efd->erd", expert_hidden, expert_down, preferred_element_type=jnp.float32
    )
    expert_result = expert_result.astype(jnp.bfloat16)
    local_experts = expert_result.shape[0]
    expert_result = expert_result.reshape(1, local_experts, ep_count, CAP, slice_width)
    returned = lax.all_to_all(expert_result, "ep", split_axis=2, concat_axis=0, tiled=True).reshape(
        EXPERTS * CAP, slice_width
    )
    route_gates = route_weights / jnp.sum(route_weights, axis=-1, keepdims=True)
    weighted = placed.astype(jnp.float32) * route_gates.reshape(-1)[None, :]
    combine_matrix = jnp.sum(weighted.T.reshape(seq_count, TOPK, EXPERTS * CAP), axis=1)
    expert_mix = jnp.dot(
        combine_matrix, returned.astype(jnp.float32), precision=lax.Precision.HIGHEST
    )
    dense_hidden = (jax.nn.silu(dense_pre_gate) * dense_pre_up).astype(jnp.bfloat16)
    dense_part = jnp.dot(dense_hidden, dense_down, preferred_element_type=jnp.float32)
    dense_out = widened(sent_and_summed(dense_part.astype(jnp.bfloat16), "ep", 0))
    mix_gate = jax.nn.sigmoid(jnp.dot(hidden_in, dense_mix, preferred_element_type=jnp.float32))
    combined = (
        residual_scale * own_cols.astype(jnp.float32) + expert_mix + mix_gate[:, None] * dense_out
    )
    moments = together((jnp.sum(combined, axis=1), jnp.sum(combined * combined, axis=1)), "tp")
    average = moments[0] / model_width
    variance = moments[1] / model_width - average * average
    layer_out = (
        (combined - average[:, None]) * lax.rsqrt(variance + layer_epsilon)[:, None] * second_gain
    )
    return layer_out.astype(jnp.bfloat16)


def solution(mesh):
    return jax.shard_map(
        on_device,
        mesh=mesh,
        in_specs=(
            P("ep", None),
            P("ep", "tp"),
            P("ep", "tp"),
            P("ep", "tp"),
            P("tp", "ep"),
            P("tp"),
            P(),
            P("ep", None, "tp", None),
            P("ep", None, "tp", None),
            P("ep"),
            P(),
            P("tp"),
            P("ep", None),
            P("ep", None),
            P("ep", "tp", None),
            P("ep", "tp", None),
            P("ep", None, "tp"),
            P("tp", "ep"),
            P("tp", "ep"),
            P("ep", "tp"),
            P(),
        ),
        out_specs=P("ep", "tp"),
        check_vma=False,
    )
```

profile of v0, /device:TPU:1, one launch (start us, length us, event | category | flops | bytes accessed | tf_op | source)
XLA Modules:
  0.0 302.1 jit_solution(6328532575109537820)
XLA Ops:
  6.5 1.6 copy.150
  8.2 7.6 %all-to-all-start = ((bf16[16,16,256]{2,0,1:T(8,128)(2,1)}), bf16[16,16,256]{2,0,1:T(8,128)(2,1)S(1)}, u32[]{:S(2)}, u32[]{:S(2)}) async-start(bf16[16,16,256]{2,0,1:T(8,128)(2,1)} %bitcast.183), calls=%async_computation | async-start | bytes 262144 | tf_op jit(solution)/shard_map/all_to_all | solution.py:166
  15.8 0.7 iota_compare_fusion
  16.5 6.1 %all-to-all-done = bf16[16,16,256]{2,0,1:T(8,128)(2,1)S(1)} async-done(((bf16[16,16,256]{2,0,1:T(8,128)(2,1)}), bf16[16,16,256]{2,0,1:T(8,128)(2,1)S(1)}, u32[]{:S(2)}, u32[]{:S(2)}) %all-to-all-start) | async-done | bytes 131104 | tf_op jit(solution)/shard_map/all_to_all | solution.py:166
  22.6 1.1 convolution_convert_fusion.4
  23.7 1.0 convolution_convert_fusion.7
  24.7 1.0 convolution_convert_fusion.8
  25.8 0.7 pad_maximum_fusion.1
  26.5 3.5 %all-to-all-start.1 = ((bf16[16,16,512]{2,1,0:T(8,128)(2,1)}), bf16[16,16,512]{2,1,0:T(8,128)(2,1)S(1)}, u32[]{:S(2)}, u32[]{:S(2)}) async-start(bf16[16,16,512]{2,1,0:T(8,128)(2,1)} %pad_maximum_fusion.1), calls=%async_computation.1 | async-start | bytes 524288 | tf_op jit(solution)/shard_map/all_to_all | solution.py:30
  30.1 0.7 convert_element_type.137
  30.7 6.4 %copy.104 = bf16[16,1024,1,128]{1,3,0,2:T(8,128)(2,1)} copy(bf16[16,1024,1,128]{3,1,2,0:T(8,128)(2,1)} %param.28) | data formatting | bytes 8388608 | tf_op args[7]
  37.1 0.1 multiply_cosine_fusion
  37.3 0.3 all-to-all-done.1
  37.7 0.1 reshape.492
  37.8 0.1 fusion.57
  37.9 0.1 fusion.47
  38.1 0.2 fusion.45
  38.3 0.1 copy.119
  38.4 3.0 %fusion.60 = (f32[16,2,2]{1,2,0:T(2,128)S(1)}, f32[16,1,2,2,1024]{4,2,3,0,1:T(2,128)S(1)}) fusion(bf16[16,1024,2,64]{1,3,2,0:T(8,128)(2,1)} %bitcast.185, bf16[16,2,2,32]{3,1,2,0:T(2,128)(2,1)S(1)} %get-tuple-element.10, bf16[16,2,2,32]{3,1,2,0:T(2,128)(2,1)S(1)} %get-tuple-element.9, pred[16,1024]{1,0:T(8,128)(4,1)S(1)} %iota_compare_fusion), kind=kOutput, calls=%fused_computation.122 | convolution fusion | flops 8601536 | bytes 4481280 | tf_op jit(solution)/shard_map/skgcd,sjkcd->skgcj/dot_general | solution.py:107
  41.5 0.1 copy.105
  41.6 0.1 copy.107
  41.7 0.3 fusion.23
  42.0 0.1 copy.108
  42.1 0.1 copy.109
  42.2 0.3 fusion.22
  42.8 3.0 multiply_reduce_fusion.2
  45.8 0.1 multiply_convert_fusion.4
  45.9 13.1 %all_to_all.79 = bf16[16,16,256]{2,1,0:T(8,128)(2,1)S(1)} all-to-all(bf16[16,16,256]{2,1,0:T(8,128)(2,1)S(1)} %broadcast_in_dim.22), channel_id=1, replica_groups=mesh['ep'=16,'tp'=16] {'ep'}, dimensions={0} | all-to-all | bytes 262144 | tf_op jit(solution)/shard_map/all_to_all | solution.py:36
  59.0 0.8 convolution_convert_fusion.3
  60.0 0.1 eq.37
  60.2 0.2 select_reduce_fusion.1
  60.5 0.1 copy.114
  60.6 41.6 %all-gather.3.cloned.1.call-done = bf16[4096,256]{1,0:T(8,128)(2,1)} async-done(((bf16[256,256]{1,0:T(8,128)(2,1)}), bf16[4096,256]{1,0:T(8,128)(2,1)}) %all-gather.3.cloned.1.call-update) | async-done | bytes 2097168 | tf_op jit(solution)/shard_map/all_gather | solution.py:51
  102.2 2.6 reduce_sum.131
  104.8 6.5 %all-to-all-start.3 = ((bf16[16,16,256]{2,1,0:T(8,128)(2,1)}), bf16[16,16,256]{2,1,0:T(8,128)(2,1)S(1)}, u32[]{:S(2)}, u32[]{:S(2)}) async-start(bf16[16,16,256]{2,1,0:T(8,128)(2,1)} %bitcast.28), calls=%async_computation.3 | async-start | bytes 262144 | tf_op jit(solution)/shard_map/all_to_all | solution.py:188
  111.4 6.8 %all-to-all-done.3 = bf16[16,16,256]{2,1,0:T(8,128)(2,1)S(1)} async-done(((bf16[16,16,256]{2,1,0:T(8,128)(2,1)}), bf16[16,16,256]{2,1,0:T(8,128)(2,1)S(1)}, u32[]{:S(2)}, u32[]{:S(2)}) %all-to-all-start.3) | async-done | bytes 131104 | tf_op jit(solution)/shard_map/all_to_all | solution.py:188
  118.2 0.2 fusion.21
  118.4 0.2 multiply_reduce_fusion
  118.6 0.1 multiply_convert_fusion.2
  118.8 0.1 convolution_convert_fusion.10
  118.9 0.6 reshape.478
  119.5 3.5 %all-to-all-start.4 = ((bf16[16,1,4,256]{3,2,1,0:T(4,128)(2,1)}), bf16[16,1,4,256]{3,2,1,0:T(4,128)(2,1)S(1)}, u32[]{:S(2)}, u32[]{:S(2)}) async-start(bf16[16,1,4,256]{3,2,1,0:T(4,128)(2,1)} %bitcast.30), calls=%async_computation.4 | async-start | bytes 65536 | tf_op jit(solution)/shard_map/all_to_all | solution.py:211
  123.1 6.3 %all-to-all-done.4 = bf16[16,1,4,256]{3,2,1,0:T(4,128)(2,1)S(1)} async-done(((bf16[16,1,4,256]{3,2,1,0:T(4,128)(2,1)}), bf16[16,1,4,256]{3,2,1,0:T(4,128)(2,1)S(1)}, u32[]{:S(2)}, u32[]{:S(2)}) %all-to-all-start.4) | async-done | bytes 32800 | tf_op jit(solution)/shard_map/all_to_all | solution.py:211
  129.4 0.6 broadcast_in_dim.24
  130.1 3.5 %all-to-all-start.5 = ((bf16[16,16,256]{2,1,0:T(8,128)(2,1)}), bf16[16,16,256]{2,1,0:T(8,128)(2,1)S(1)}, u32[]{:S(2)}, u32[]{:S(2)}) async-start(bf16[16,16,256]{2,1,0:T(8,128)(2,1)} %broadcast_in_dim.24), calls=%async_computation.5 | async-start | bytes 262144 | tf_op jit(solution)/shard_map/all_to_all | solution.py:36
  133.7 0.3 fusion.2
  134.0 0.3 fusion.3
  134.4 6.0 %all-to-all-done.5 = bf16[16,16,256]{2,1,0:T(8,128)(2,1)S(1)} async-done(((bf16[16,16,256]{2,1,0:T(8,128)(2,1)}), bf16[16,16,256]{2,1,0:T(8,128)(2,1)S(1)}, u32[]{:S(2)}, u32[]{:S(2)}) %all-to-all-start.5) | async-done | bytes 131104 | tf_op jit(solution)/shard_map/all_to_all | solution.py:36
  140.4 0.2 fusion.7
  140.6 0.2 fusion.8
  140.8 0.9 pad_maximum_fusion
  141.8 109.3 %all-reduce.2.cloned.1.call-done = bf16[327680]{0:T(1024)(128)(2,1)} async-done(((bf16[327680]{0:T(1024)(128)(2,1)}), bf16[327680]{0:T(1024)(128)(2,1)}) %all-reduce.2.cloned.1.call-update) | async-done | bytes 655376 | tf_op jit(solution)/shard_map/psum | solution.py:58
  251.1 1.1 slice_convert_fusion.1
  252.4 1.5 convolution_convert_fusion.9
  253.9 0.6 reshape.488
  254.6 6.5 %all-to-all-start.6 = ((bf16[1,1,16,4,256]{4,3,1,0,2:T(4,128)(2,1)}), bf16[1,1,16,4,256]{4,3,1,0,2:T(4,128)(2,1)S(1)}, u32[]{:S(2)}, u32[]{:S(2)}) async-start(bf16[1,1,16,4,256]{4,3,1,0,2:T(4,128)(2,1)} %bitcast.37), calls=%async_computation.6 | async-start | bytes 65536 | tf_op jit(solution)/shard_map/all_to_all | solution.py:242
  261.1 1.7 convolution_convert_fusion.2
  262.8 4.8 %all-to-all-done.6 = bf16[1,1,16,4,256]{4,3,1,0,2:T(4,128)(2,1)S(1)} async-done(((bf16[1,1,16,4,256]{4,3,1,0,2:T(4,128)(2,1)}), bf16[1,1,16,4,256]{4,3,1,0,2:T(4,128)(2,1)S(1)}, u32[]{:S(2)}, u32[]{:S(2)}) %all-to-all-start.6) | async-done | bytes 32800 | tf_op jit(solution)/shard_map/all_to_all | solution.py:242
  267.6 3.5 %all-to-all-start.7 = ((bf16[16,16,256]{2,1,0:T(8,128)(2,1)}), bf16[16,16,256]{2,1,0:T(8,128)(2,1)S(1)}, u32[]{:S(2)}, u32[]{:S(2)}) async-start(bf16[16,16,256]{2,1,0:T(8,128)(2,1)} %bitcast.42), calls=%async_computation.7 | async-start | bytes 262144 | tf_op jit(solution)/shard_map/all_to_all | solution.py:30
  271.1 0.2 fusion.16
  271.3 6.6 %all-to-all-done.7 = bf16[16,16,256]{2,1,0:T(8,128)(2,1)S(1)} async-done(((bf16[16,16,256]{2,1,0:T(8,128)(2,1)}), bf16[16,16,256]{2,1,0:T(8,128)(2,1)S(1)}, u32[]{:S(2)}, u32[]{:S(2)}) %all-to-all-start.7) | async-done | bytes 131104 | tf_op jit(solution)/shard_map/all_to_all | solution.py:30
  277.9 0.2 fusion.56
  278.3 16.3 %all_to_all.80 = f32[16,1,32]{2,1,0:T(1,128)S(1)} all-to-all(f32[16,1,32]{2,1,0:T(1,128)S(1)} %broadcast_in_dim.25), channel_id=1, replica_groups=mesh['ep'=16,'tp'=16] {'tp'}, dimensions={0} | all-to-all | bytes 4096 | tf_op jit(solution)/shard_map/all_to_all | solution.py:36
  294.6 0.7 multiply_convert_fusion.3
  (77 shorter events, 1.7 us)
Async XLA Ops:
  6.5 127.1 %copy-start = (bf16[1,256,2048]{2,1,0:T(8,128)(2,1)S(1)}, bf16[1,256,2048]{2,1,0:T(8,128)(2,1)}, u32[]{:S(2)}) copy-start(bf16[1,256,2048]{2,1,0:T(8,128)(2,1)} %param.35) | copy-start | bytes 3145732
  8.2 14.4 %all-to-all-start = ((bf16[16,16,256]{2,0,1:T(8,128)(2,1)}), bf16[16,16,256]{2,0,1:T(8,128)(2,1)S(1)}, u32[]{:S(2)}, u32[]{:S(2)}) async-start(bf16[16,16,256]{2,0,1:T(8,128)(2,1)} %bitcast.183), calls=%async_computation | async-start | bytes 262144 | tf_op jit(solution)/shard_map/all_to_all | solution.py:166
  26.5 11.0 %all-to-all-start.1 = ((bf16[16,16,512]{2,1,0:T(8,128)(2,1)}), bf16[16,16,512]{2,1,0:T(8,128)(2,1)S(1)}, u32[]{:S(2)}, u32[]{:S(2)}) async-start(bf16[16,16,512]{2,1,0:T(8,128)(2,1)} %pad_maximum_fusion.1), calls=%async_computation.1 | async-start | bytes 524288 | tf_op jit(solution)/shard_map/all_to_all | solution.py:30
  30.0 72.2 %all-gather.3.cloned.1.call-start = ((), (), s32[]{:S(2)}) async-start(), calls=%async_computation.10 | async-start | bytes 2228224 | tf_op jit(solution)/shard_map/all_gather | solution.py:51
  37.1 5.4 %copy-start.10 = (f32[2]{0:T(128)S(1)}, f32[2]{0:T(128)}, u32[]{:S(2)}) copy-start(f32[2]{0:T(128)} %param.26) | copy-start | bytes 28
  38.4 7.3 %copy-start.12 = (f32[128]{0:T(128)S(1)}, f32[128]{0:T(128)}, u32[]{:S(2)}) copy-start(f32[128]{0:T(128)} %param.27) | copy-start | bytes 1540
  38.4 20.6 %copy-start.3 = (bf16[256,256]{1,0:T(8,128)(2,1)S(1)}, bf16[256,256]{1,0:T(8,128)(2,1)}, u32[]{:S(2)}) copy-start(bf16[256,256]{1,0:T(8,128)(2,1)} %param.25) | copy-start | bytes 393220
  41.5 18.4 %copy-start.8 = (s32[16,2]{0,1:T(2,128)S(1)}, s32[16,2]{0,1:T(2,128)}, u32[]{:S(2)}) copy-start(s32[16,2]{0,1:T(2,128)} %param.33) | copy-start | bytes 388
  42.5 75.7 %copy-start.1 = (bf16[16,4096]{1,0:T(8,128)(2,1)S(1)}, bf16[16,4096]{1,0:T(8,128)(2,1)}, u32[]{:S(2)}) copy-start(bf16[16,4096]{1,0:T(8,128)(2,1)} %param.21) | copy-start | bytes 393220
  42.7 75.9 %copy-start.6 = (f32[4096]{0:T(1024)S(1)}, f32[4096]{0:T(1024)}, u32[]{:S(2)}) copy-start(f32[4096]{0:T(1024)} %param.31) | copy-start | bytes 49156
  42.7 80.3 %copy-start.7 = (bf16[4096]{0:T(1024)(128)(2,1)S(1)}, bf16[4096]{0:T(1024)(128)(2,1)}, u32[]{:S(2)}) copy-start(bf16[4096]{0:T(1024)(128)(2,1)} %param.41) | copy-start | bytes 24580
  42.7 80.3 %copy-start.9 = (f32[16,2]{0,1:T(2,128)S(1)}, f32[16,2]{0,1:T(2,128)}, u32[]{:S(2)}) copy-start(f32[16,2]{0,1:T(2,128)} %param.34) | copy-start | bytes 388
  45.8 88.3 %copy-start.2 = (bf16[1,256,2048]{2,1,0:T(8,128)(2,1)S(1)}, bf16[1,256,2048]{2,1,0:T(8,128)(2,1)}, u32[]{:S(2)}) copy-start(bf16[1,256,2048]{2,1,0:T(8,128)(2,1)} %param.36) | copy-start | bytes 3145732
  59.9 80.5 %copy-start.4 = (bf16[256,128]{1,0:T(8,128)(2,1)S(1)}, bf16[256,128]{1,0:T(8,128)(2,1)}, u32[]{:S(2)}) copy-start(bf16[256,128]{1,0:T(8,128)(2,1)} %param.39) | copy-start | bytes 196612
  102.2 38.4 %copy-start.5 = (bf16[256,128]{1,0:T(8,128)(2,1)S(1)}, bf16[256,128]{1,0:T(8,128)(2,1)}, u32[]{:S(2)}) copy-start(bf16[256,128]{1,0:T(8,128)(2,1)} %param.38) | copy-start | bytes 196612
  104.8 13.4 %all-to-all-start.3 = ((bf16[16,16,256]{2,1,0:T(8,128)(2,1)}), bf16[16,16,256]{2,1,0:T(8,128)(2,1)S(1)}, u32[]{:S(2)}, u32[]{:S(2)}) async-start(bf16[16,16,256]{2,1,0:T(8,128)(2,1)} %bitcast.28), calls=%async_computation.3 | async-start | bytes 262144 | tf_op jit(solution)/shard_map/all_to_all | solution.py:188
  119.5 9.9 %all-to-all-start.4 = ((bf16[16,1,4,256]{3,2,1,0:T(4,128)(2,1)}), bf16[16,1,4,256]{3,2,1,0:T(4,128)(2,1)S(1)}, u32[]{:S(2)}, u32[]{:S(2)}) async-start(bf16[16,1,4,256]{3,2,1,0:T(4,128)(2,1)} %bitcast.30), calls=%async_computation.4 | async-start | bytes 65536 | tf_op jit(solution)/shard_map/all_to_all | solution.py:211
  130.1 10.3 %all-to-all-start.5 = ((bf16[16,16,256]{2,1,0:T(8,128)(2,1)}), bf16[16,16,256]{2,1,0:T(8,128)(2,1)S(1)}, u32[]{:S(2)}, u32[]{:S(2)}) async-start(bf16[16,16,256]{2,1,0:T(8,128)(2,1)} %broadcast_in_dim.24), calls=%async_computation.5 | async-start | bytes 262144 | tf_op jit(solution)/shard_map/all_to_all | solution.py:36
  133.6 117.5 %all-reduce.2.cloned.1.call-start = ((), (), s32[]{:S(2)}) async-start(), calls=%async_computation.9 | async-start | bytes 1310720 | tf_op jit(solution)/shard_map/psum | solution.py:58
  140.8 120.4 %copy-start.13 = (bf16[128,256]{1,0:T(8,128)(2,1)S(1)}, bf16[128,256]{1,0:T(8,128)(2,1)}, u32[]{:S(2)}) copy-start(bf16[128,256]{1,0:T(8,128)(2,1)} %param.40) | copy-start | bytes 196612
  141.8 152.8 %copy-start.11 = (f32[256]{0:T(256)S(1)}, f32[256]{0:T(256)}, u32[]{:S(2)}) copy-start(f32[256]{0:T(256)} %param.32) | copy-start | bytes 3076
  254.6 13.0 %all-to-all-start.6 = ((bf16[1,1,16,4,256]{4,3,1,0,2:T(4,128)(2,1)}), bf16[1,1,16,4,256]{4,3,1,0,2:T(4,128)(2,1)S(1)}, u32[]{:S(2)}, u32[]{:S(2)}) async-start(bf16[1,1,16,4,256]{4,3,1,0,2:T(4,128)(2,1)} %bitcast.37), calls=%async_computation.6 | async-start | bytes 65536 | tf_op jit(solution)/shard_map/all_to_all | solution.py:242
  267.6 10.3 %all-to-all-start.7 = ((bf16[16,16,256]{2,1,0:T(8,128)(2,1)}), bf16[16,16,256]{2,1,0:T(8,128)(2,1)S(1)}, u32[]{:S(2)}, u32[]{:S(2)}) async-start(bf16[16,16,256]{2,1,0:T(8,128)(2,1)} %bitcast.42), calls=%async_computation.7 | async-start | bytes 262144 | tf_op jit(solution)/shard_map/all_to_all | solution.py:30
Sparse Core Ops, SparseCore 0:
  60.0 42.1 all-gather.2
  141.8 109.2 all-reduce.1
where the time goes:
time: 303 us; the launch traced here: 302 us
  waiting for transfers between devices  188 us (62%)
  starting transfers between devices  34.8 us (11%)
  blocking collectives  29.4 us (10%)
  matrix products  14.9 us (5%)
  between operations  13.9 us (5%)
  local copies, waits for them, and re-layouts  11.5 us (4%)
  other arithmetic  9.75 us (3%)
    psum x1, waiting for transfers between devices, packed_total(): so_far = lax.psum(jnp.concatenate([a.ravel() for a in arrays]), axis)  109 us
    all_gather x1, waiting for transfers between devices, over_pieces(): return lax.all_gather(shard, axis).astype(jnp.float32).sum(0)  41.6 us
    all_to_all x2, blocking collectives, sent_to_all(): return lax.all_to_all(copies, axis, split_axis=0, concat_axis=0, tiled=True)  29.4 us
    all_to_all x1, starting transfers between devices, on_device(): lax.all_to_all(tokens, 'ep', split_axis=1, concat_axis=0, tiled=True)  7.57 us
    all_to_all x2, starting transfers between devices, sent_and_summed(): lax.all_to_all(tiles, axis, split_axis=0, concat_axis=0, tiled=True)  7.04 us
    all_to_all x2, waiting for transfers between devices, sent_and_summed(): lax.all_to_all(tiles, axis, split_axis=0, concat_axis=0, tiled=True)  6.87 us
    all_to_all x1, waiting for transfers between devices, on_device(): lax.all_to_all(column_part.astype(jnp.bfloat16), 'ep', split_axis=0, conc...  6.83 us
    unnamed x34, local copies, waits for them, and re-layouts  6.63 us
  transfers between devices with their start and end apart: 9, of which 9 were waited for; matrix products, arithmetic and copies ran while one was open for 4% of the time, Pallas kernels for 0%

commit v1 on v0

v1 whole, which is shorter than its diff:
```python
import functools
import math

import jax
import jax.numpy as jnp
from jax import lax
from jax.experimental import pallas as pl
from jax.experimental.pallas import tpu as pltpu
from jax.sharding import PartitionSpec as P

N = 16
CACHE = 1024
CAP = 4
F32 = jnp.float32
BF16 = jnp.bfloat16
MESH = pl.DeviceIdType.MESH

PA, PMETA, PB, PD, PE, PF, PG, PMIX, PH, PI, PI2, PJ, PK = range(13)
PHASES = 13

LOCALS = (
    "tok", "qw", "kw", "vw", "ow", "lam", "hgain", "kc", "vc", "lens", "fgain",
    "sgain", "ids", "rw", "eg", "eu", "ed", "dg", "du", "dd", "dmix",
)


def dot(a, b):
    return jnp.dot(a, b, preferred_element_type=F32)


def to_column(row, n):
    same = lax.broadcasted_iota(jnp.int32, (n, n), 0) == lax.broadcasted_iota(jnp.int32, (n, n), 1)
    return jnp.sum(jnp.where(same, jnp.broadcast_to(row, (n, n)), 0), axis=1, keepdims=True)


def to_row(column, n, lanes):
    same = lax.broadcasted_iota(jnp.int32, (n, lanes), 0) == lax.broadcasted_iota(
        jnp.int32, (n, lanes), 1
    )
    return jnp.sum(jnp.where(same, jnp.broadcast_to(column, (n, lanes)), 0), axis=0, keepdims=True)


def kernel(
    tok_h, qw_h, kw_h, vw_h, ow_h, lam_h, hgain_h, kc_h, vc_h, lens_h, fgain_h, sgain_h,
    ids_h, rw_h, eg_h, eu_h, ed_h, dg_h, du_h, dd_h, dmix_h,
    out_ref,
    tok, wqkv, ow, lam, hgain, kc, vc, lens, fgain, sgain, ids, rw, wgu, ed, wd, dd, dmix,
    xcol, meta, metas, bsend, brecv, qs, kn, vn, h0, h1, lens_b, dsend, drecv, esend, erecv,
    fsend, frecv, gsend, grecv, msend, mrecv, gw, hsend, hrecv, isend, isend2, ihid, idense,
    jsend, jrecv, ksend, krecv, pick, place, gates,
    lsem, ssem, rsem, ready,
):
    e = lax.axis_index("ep")
    t = lax.axis_index("tp")

    def chunk(i, width):
        return pl.ds(pl.multiple_of(i * width, width), width)

    def bring(name, pairs):
        sem = lsem.at[LOCALS.index(name)]
        for src, dst in pairs:
            pltpu.make_async_copy(src, dst, sem).start()

    def arrived(name, whole):
        pltpu.make_async_copy(whole, whole, lsem.at[LOCALS.index(name)]).wait()

    bring("tok", [(tok_h, tok)])
    bring("ids", [(ids_h, ids)])
    bring("rw", [(rw_h, rw)])
    bring("qw", [(qw_h, wqkv.at[:, 0:256])])
    bring("kw", [(kw_h, wqkv.at[:, 256:384])])
    bring("vw", [(vw_h, wqkv.at[:, 384:512])])
    bring("lens", [(lens_h, lens)])
    bring("lam", [(lam_h, lam)])
    bring("hgain", [(hgain_h, hgain)])
    bring("kc", [(kc_h, kc)])
    bring("vc", [(vc_h, vc)])
    bring("ow", [(ow_h, ow)])
    bring("fgain", [(fgain_h, fgain)])
    bring("dmix", [(dmix_h, dmix)])
    bring("sgain", [(sgain_h, sgain)])

    def bring_pair(i, _):
        sem_g = lsem.at[LOCALS.index("eg")]
        sem_u = lsem.at[LOCALS.index("eu")]
        even = pl.ds(pl.multiple_of(i * 256, 256), 128)
        odd = pl.ds(pl.multiple_of(i * 256 + 128, 128), 128)
        pltpu.make_async_copy(eg_h.at[:, chunk(i, 128)], wgu.at[:, even], sem_g).start()
        pltpu.make_async_copy(eu_h.at[:, chunk(i, 128)], wgu.at[:, odd], sem_u).start()
        return 0

    lax.fori_loop(0, N, bring_pair, 0)
    bring("dg", [(dg_h, wd.at[:, 0:128])])
    bring("du", [(du_h, wd.at[:, 128:256])])
    bring("ed", [(ed_h, ed)])
    bring("dd", [(dd_h, dd)])

    barrier = pltpu.get_barrier_semaphore()

    def greet(k, _):
        pl.semaphore_signal(
            barrier, inc=1, device_id=(lax.rem(e + k, N), t), device_id_type=MESH
        )
        pl.semaphore_signal(
            barrier, inc=1, device_id=(e, lax.rem(t + k, N)), device_id_type=MESH
        )
        return 0

    lax.fori_loop(1, N, greet, 0)

    def send(phase, src, dst, to):
        pltpu.make_async_remote_copy(
            src_ref=src,
            dst_ref=dst,
            send_sem=ssem.at[phase],
            recv_sem=rsem.at[phase],
            device_id=to,
            device_id_type=MESH,
        ).start()

    def over_ep(phase, src_of, dst):
        def one(k, _):
            a = lax.rem(e + k, N)
            send(phase, src_of(a), dst, (a, t))
            return 0

        lax.fori_loop(1, N, one, 0)

    def over_tp(phase, src_of, dst):
        def one(k, _):
            b = lax.rem(t + k, N)
            send(phase, src_of(b), dst, (e, b))
            return 0

        lax.fori_loop(1, N, one, 0)

    def received(phase, blocks):
        pltpu.make_async_copy(blocks, blocks, rsem.at[phase]).wait()

    def sent(phase, blocks):
        pltpu.make_async_copy(blocks, blocks, ssem.at[phase]).wait()

    lane = lax.broadcasted_iota(jnp.int32, (N, 128), 1)

    arrived("ids", ids)
    arrived("rw", rw)
    id0 = to_column(ids[0:1, :], N)
    id1 = to_column(ids[1:2, :], N)
    w0 = to_column(rw[0:1, :], N)
    w1 = to_column(rw[1:2, :], N)
    total = w0 + w1
    hit0 = lane == id0
    hit1 = lane == id1
    hit = jnp.where(hit0 | hit1, 1.0, 0.0).astype(F32)
    before = jnp.where(
        lax.broadcasted_iota(jnp.int32, (N, N), 1) < lax.broadcasted_iota(jnp.int32, (N, N), 0),
        1.0,
        0.0,
    ).astype(F32)
    slot = dot(before.astype(BF16), hit.astype(BF16))
    code = jnp.where(hit > 0.5, slot, -1.0)
    gate0 = jnp.where(lane - N == id0, w0 / total, 0.0)
    gate1 = jnp.where(lane - N == id1, w1 / total, 0.0)
    meta[...] = jnp.where(lane < N, code, gate0 + gate1)
    metas[e] = meta[...]

    arrived("tok", tok)
    xcol[e] = tok[:, chunk(e, 256)]

    pl.semaphore_wait(barrier, 2 * (N - 1))

    over_ep(PA, lambda a: tok.at[:, chunk(a, 256)], xcol.at[e])
    over_ep(PMETA, lambda a: meta, metas.at[e])

    def tell(k, _):
        pl.semaphore_signal(ready, inc=1, device_id=(e, lax.rem(t + k, N)), device_id_type=MESH)
        return 0

    lax.fori_loop(1, N, tell, 0)

    arrived("lens", lens)
    length = to_column(lens[...], N)
    lens_b[...] = jnp.broadcast_to(length, (N, 128))
    turn = lax.rem(lane, 32).astype(F32) * (2.0 / 64)
    angle = length.astype(F32) * jnp.exp(turn * (-math.log(500000.0)))
    low = lax.rem(lane, 64) < 32
    cosine = jnp.cos(angle)
    sine = jnp.sin(angle)
    sine = jnp.where(low, -sine, sine)

    arrived("qw", wqkv.at[:, 0:256])
    arrived("kw", wqkv.at[:, 256:384])
    arrived("vw", wqkv.at[:, 384:512])
    received(PA, xcol.at[0:15])
    bsend[...] = dot(xcol[...].reshape(256, 256), wqkv[...]).astype(BF16).reshape(N, N, 512)
    brecv[e] = bsend[e]
    over_ep(PB, lambda a: bsend.at[a], brecv.at[e])

    received(PMETA, metas.at[0:15])
    every = metas[...].reshape(256, 128)
    wide_lane = lax.broadcasted_iota(jnp.int32, (256, 128), 1)
    code_col = jnp.sum(jnp.where(wide_lane == e, every, 0.0), axis=1, keepdims=True)
    gate_col = jnp.sum(jnp.where(wide_lane == e + N, every, 0.0), axis=1, keepdims=True)
    block = (lax.broadcasted_iota(jnp.int32, (256, 1), 0) // N * CAP).astype(F32)
    target = jnp.where(code_col >= 0.0, code_col + block, -1.0)
    place[...] = jnp.where(
        lax.broadcasted_iota(jnp.int32, (256, 64), 1).astype(F32) == target, 1.0, 0.0
    ).astype(BF16)
    pick[...] = jnp.where(
        lax.broadcasted_iota(jnp.int32, (64, 256), 0).astype(F32) == to_row(target, 256, 256),
        1.0,
        0.0,
    ).astype(BF16)
    gates[...] = gate_col

    received(PB, brecv.at[0:15])
    qkv = jnp.sum(brecv[...].astype(F32), axis=0).astype(BF16).astype(F32)

    def rotated(x):
        swapped = jnp.where(low, pltpu.roll(x, 96, 1), pltpu.roll(x, 32, 1))
        return (x * cosine + swapped * sine).astype(BF16).astype(F32)

    first = lane < 64
    qs[...] = jnp.zeros_like(qs)
    for g in range(2):
        q = rotated(qkv[:, g * 128 : (g + 1) * 128]) * 0.125
        qs[pl.ds(g, N, stride=8), :] = jnp.where(first, q, 0.0)
        qs[pl.ds(g + 4, N, stride=8), :] = jnp.where(first, 0.0, q)
    kn[...] = rotated(qkv[:, 256:384])
    vn[...] = qkv[:, 384:512]

    arrived("lam", lam)
    row8 = lax.broadcasted_iota(jnp.int32, (8, 1), 0)
    share = jnp.where(row8 == 4, -lam[0:1, 0:1], jnp.where(row8 == 5, -lam[0:1, 1:2], 1.0))
    place_of = lax.broadcasted_iota(jnp.int32, (8, CACHE), 1)

    arrived("kc", kc)
    arrived("vc", vc)

    def attend(s):
        q = qs[pl.ds(pl.multiple_of(s * 8, 8), 8), :]
        scores = lax.dot_general(
            q.astype(BF16), kc[s], (((1,), (1,)), ((), ())), preferred_element_type=F32
        )
        fresh = jnp.sum(q * kn[pl.ds(s, 1), :], axis=1, keepdims=True)
        scores = jnp.where(place_of < lens_b[pl.ds(s, 1), 0:1], scores, -1e30)
        top = jnp.maximum(jnp.max(scores, axis=1, keepdims=True), fresh)
        p = jnp.exp(scores - top)
        fresh_p = jnp.exp(fresh - top)
        scale = share / (jnp.sum(p, axis=1, keepdims=True) + fresh_p)
        p = p * scale
        fresh_p = fresh_p * scale
        p = p + pltpu.roll(p, 4, 0)
        fresh_p = jnp.broadcast_to(fresh_p, (8, 128))
        fresh_p = (fresh_p + pltpu.roll(fresh_p, 4, 0)).astype(BF16).astype(F32)
        head = dot(p.astype(BF16), vc[s]) + fresh_p * vn[pl.ds(s, 1), :]
        h0[pl.ds(s, 1), :] = head[0:1, :]
        h1[pl.ds(s, 1), :] = head[1:2, :]

    def attend_some(i, _):
        for j in range(4):
            attend(i * 4 + j)
        return 0

    lax.fori_loop(0, N // 4, attend_some, 0)

    arrived("hgain", hgain)
    for g, ref in enumerate((h0, h1)):
        head = ref[...]
        mean = jnp.mean(head * head, axis=1, keepdims=True)
        head = head * lax.rsqrt(mean + 1e-6) * hgain[...] * 0.8
        dsend[:, g * 128 : (g + 1) * 128] = head.astype(BF16)
    drecv[e] = dsend[...]
    over_ep(PD, lambda a: dsend, drecv.at[e])

    arrived("ow", ow)
    arrived("fgain", fgain)
    arrived("dmix", dmix)
    gw[...] = fgain[...] * dmix[...].astype(F32)

    def block_of(ref):
        return jnp.concatenate([ref[pl.ds(2 * t, 1), :], ref[pl.ds(2 * t + 1, 1), :]], axis=1)

    gain = block_of(fgain)
    gain_mix = block_of(gw)
    pl.semaphore_wait(ready, N - 1)
    received(PD, drecv.at[0:15])
    esend[...] = dot(drecv[...].reshape(256, 256), ow[...]).astype(BF16).reshape(N, N, 256)

    def spread(k, _):
        a = lax.rem(e + k, N)
        send(PE, esend.at[a], erecv.at[t], (a, e))
        return 0

    lax.fori_loop(1, N, spread, 0)

    @pl.when(e == t)
    def _():
        pltpu.make_async_copy(esend.at[e], erecv.at[t], rsem.at[PE]).start()

    @pl.when(e != t)
    def _():
        send(PE, esend.at[e], erecv.at[t], (e, e))

    received(PE, erecv)
    root = 2.0**0.5
    attention = jnp.sum(erecv[...].astype(F32), axis=0).astype(BF16).astype(F32)
    residual = root * tok[:, chunk(t, 256)].astype(F32) + attention

    def block_moments(x):
        mean = jnp.sum(x, axis=1, keepdims=True) * (1.0 / 256)
        centred = x - mean
        return mean, centred, jnp.sum(centred * centred, axis=1, keepdims=True)

    mean_b, centred, square_b = block_moments(residual)
    mixed_b = jnp.sum(centred * gain_mix, axis=1, keepdims=True)
    gain_b = jnp.sum(gain_mix, axis=1, keepdims=True)
    fsend[0:1, :] = to_row(mean_b, N, 128)
    fsend[1:2, :] = to_row(square_b, N, 128)
    fsend[2:3, :] = to_row(mixed_b, N, 128)
    fsend[3:4, :] = jnp.broadcast_to(gain_b, (1, 128))
    frecv[t] = fsend[...]
    over_tp(PF, lambda b: fsend, frecv.at[t])
    received(PF, frecv.at[0:15])

    def whole_moments(means, squares):
        mean = jnp.sum(means, axis=0, keepdims=True) * (1.0 / N)
        apart = means - mean
        variance = (
            jnp.sum(squares, axis=0, keepdims=True)
            + 256.0 * jnp.sum(apart * apart, axis=0, keepdims=True)
        ) * (1.0 / 4096)
        return mean, apart, lax.rsqrt(variance + 1e-5)

    means = frecv[:, 0, :]
    mean, apart, scale = whole_moments(means, frecv[:, 1, :])
    mix = scale * jnp.sum(frecv[:, 2, :] + apart * frecv[:, 3, :], axis=0, keepdims=True)
    mix = 1.0 / (1.0 + jnp.exp(-mix))
    msend[...] = jnp.broadcast_to(mix, (2, 128))
    mrecv[e] = msend[...]
    hidden = (residual - to_column_of(mean)) * to_column_of(scale) * gain
    gsend[...] = hidden.astype(BF16)
    grecv[e] = gsend[...]
    over_ep(PG, lambda a: gsend, grecv.at[e])
    over_ep(PMIX, lambda a: msend, mrecv.at[e])

    arrived("eg", wgu.at[:, 0:2048])
    arrived("eu", wgu.at[:, 2048:4096])
    arrived("dg", wd.at[:, 0:128])
    arrived("du", wd.at[:, 128:256])
    received(PG, grecv.at[0:15])
    rows = grecv[...].reshape(256, 256)
    routed = dot(pick[...], rows).astype(BF16)
    hsend[:, 64:80, :] = dot(rows, wd[...]).astype(BF16).reshape(N, N, 256)

    def partial(b):
        hsend[b, 0:64, :] = dot(routed, wgu[:, chunk(b, 256)]).astype(BF16)

    def project(k, _):
        b = lax.rem(t + k, N)
        partial(b)
        send(PH, hsend.at[b], hrecv.at[t], (e, b))
        return 0

    lax.fori_loop(1, N, project, 0)
    partial(t)
    hrecv[t] = hsend[t]
    received(PH, hrecv.at[0:15])
    pre = jnp.sum(hrecv[...].astype(F32), axis=0)
    pre_gate = pre[:, 0:128]
    active = (pre_gate / (1.0 + jnp.exp(-pre_gate)) * pre[:, 128:256]).astype(BF16)
    isend[...] = active[0:64, :]
    isend2[...] = active[64:80, :]
    ihid[:, chunk(t, 128)] = isend[...]
    idense[t] = isend2[...]
    over_tp(PI, lambda b: isend, ihid.at[:, chunk(t, 128)])
    over_tp(PI2, lambda b: isend2, idense.at[t])

    received(PMIX, mrecv.at[0:15])
    mixes = mrecv[:, 0:1, :]
    own = lax.broadcasted_iota(jnp.int32, (N, N, 128), 1) == lax.broadcasted_iota(
        jnp.int32, (N, N, 128), 2
    )
    mix_col = jnp.sum(
        jnp.where(own, jnp.broadcast_to(mixes, (N, N, 128)), 0.0), axis=2, keepdims=True
    ).reshape(256, 1)

    arrived("ed", ed)
    arrived("dd", dd)
    received(PI2, idense.at[0:15])
    dense = dot(idense[...].reshape(256, 128), dd[...]) * mix_col
    received(PI, ihid.at[:, 0 : 15 * 128])
    result = dot(ihid[...], ed[...]).astype(BF16)
    mixture = dot(place[...], result) * gates[...] + dense
    jsend[...] = mixture.astype(BF16).reshape(N, N, 256)
    jrecv[e] = jsend[e]
    over_ep(PJ, lambda a: jsend.at[a], jrecv.at[e])
    arrived("sgain", sgain)
    received(PJ, jrecv.at[0:15])
    combined = root * gsend[...].astype(F32) + jnp.sum(jrecv[...].astype(F32), axis=0)

    mean_b, _, square_b = block_moments(combined)
    ksend[0:1, :] = to_row(mean_b, N, 128)
    ksend[1:2, :] = to_row(square_b, N, 128)
    krecv[t] = ksend[...]
    over_tp(PK, lambda b: ksend, krecv.at[t])
    received(PK, krecv.at[0:15])
    mean, _, scale = whole_moments(krecv[:, 0, :], krecv[:, 1, :])
    last_gain = jnp.concatenate([sgain[0:1, :], sgain[1:2, :]], axis=1)
    out_ref[...] = (
        (combined - to_column_of(mean)) * to_column_of(scale) * last_gain
    ).astype(BF16)

    sent(PA, xcol.at[0:15])
    sent(PMETA, metas.at[0:15])
    sent(PB, bsend.at[0:15])
    sent(PD, drecv.at[0:15])
    sent(PE, esend.at[0:15])

    @pl.when(e != t)
    def _():
        sent(PE, esend.at[0])

    sent(PF, frecv.at[0:15])
    sent(PG, grecv.at[0:15])
    sent(PMIX, mrecv.at[0:15])
    sent(PH, hsend.at[0:15])
    sent(PI, ihid.at[:, 0 : 15 * 128])
    sent(PI2, idense.at[0:15])
    sent(PJ, jsend.at[0:15])
    sent(PK, krecv.at[0:15])


def to_column_of(row):
    same = lax.broadcasted_iota(jnp.int32, (N, 128), 0) == lax.broadcasted_iota(
        jnp.int32, (N, 128), 1
    )
    return jnp.sum(jnp.where(same, jnp.broadcast_to(row, (N, 128)), 0), axis=1, keepdims=True)


def on_device(
    tokens, query_weight, key_weight, value_weight, out_weight, head_lambda, head_gain,
    key_cache, value_cache, lengths, first_gain, second_gain, expert_ids, route_weights,
    expert_gate, expert_up, expert_down, dense_gate, dense_up, dense_down, dense_mix,
):
    anywhere = pl.BlockSpec(memory_space=pltpu.HBM)
    vmem = pltpu.VMEM
    scratch = [
        vmem((N, 4096), BF16),
        vmem((256, 512), BF16),
        vmem((256, 256), BF16),
        vmem((1, 2), F32),
        vmem((1, 128), F32),
        vmem((N, CACHE, 128), BF16),
        vmem((N, CACHE, 128), BF16),
        vmem((1, N), jnp.int32),
        vmem((32, 128), F32),
        vmem((2, 128), F32),
        vmem((2, N), jnp.int32),
        vmem((2, N), F32),
        vmem((256, 4096), BF16),
        vmem((2048, 256), BF16),
        vmem((256, 256), BF16),
        vmem((128, 256), BF16),
        vmem((32, 128), BF16),
        vmem((N, N, 256), BF16),
        vmem((N, 128), F32),
        vmem((N, N, 128), F32),
        vmem((N, N, 512), BF16),
        vmem((N, N, 512), BF16),
        vmem((128, 128), F32),
        vmem((N, 128), F32),
        vmem((N, 128), F32),
        vmem((N, 128), F32),
        vmem((N, 128), F32),
        vmem((N, 128), jnp.int32),
        vmem((N, 256), BF16),
        vmem((N, N, 256), BF16),
        vmem((N, N, 256), BF16),
        vmem((N, N, 256), BF16),
        vmem((4, 128), F32),
        vmem((N, 4, 128), F32),
        vmem((N, 256), BF16),
        vmem((N, N, 256), BF16),
        vmem((2, 128), F32),
        vmem((N, 2, 128), F32),
        vmem((32, 128), F32),
        vmem((N, 80, 256), BF16),
        vmem((N, 80, 256), BF16),
        vmem((64, 128), BF16),
        vmem((N, 128), BF16),
        vmem((64, 2048), BF16),
        vmem((N, N, 128), BF16),
        vmem((N, N, 256), BF16),
        vmem((N, N, 256), BF16),
        vmem((2, 128), F32),
        vmem((N, 2, 128), F32),
        vmem((64, 256), BF16),
        vmem((256, 64), BF16),
        vmem((256, 1), F32),
        pltpu.SemaphoreType.DMA((len(LOCALS),)),
        pltpu.SemaphoreType.DMA((PHASES,)),
        pltpu.SemaphoreType.DMA((PHASES,)),
        pltpu.SemaphoreType.REGULAR,
    ]
    return pl.pallas_call(
        kernel,
        out_shape=jax.ShapeDtypeStruct((N, 256), BF16),
        in_specs=[anywhere] * 21,
        out_specs=pl.BlockSpec(memory_space=pltpu.VMEM),
        scratch_shapes=scratch,
        compiler_params=pltpu.CompilerParams(
            collective_id=0, has_side_effects=True, vmem_limit_bytes=67_043_328
        ),
        name="layer",
    )(
        tokens,
        query_weight,
        key_weight,
        value_weight,
        out_weight,
        head_lambda.reshape(1, 2),
        head_gain.reshape(1, 128),
        key_cache.reshape(N, CACHE, 128),
        value_cache.reshape(N, CACHE, 128),
        lengths.reshape(1, N),
        first_gain.reshape(32, 128),
        second_gain.reshape(2, 128),
        expert_ids.T,
        route_weights.T,
        expert_gate.reshape(256, 2048),
        expert_up.reshape(256, 2048),
        expert_down.reshape(2048, 256),
        dense_gate,
        dense_up,
        dense_down,
        dense_mix.reshape(32, 128),
    )


def solution(mesh):
    return jax.shard_map(
        on_device,
        mesh=mesh,
        in_specs=(
            P("ep", None),
            P("ep", "tp"),
            P("ep", "tp"),
            P("ep", "tp"),
            P("tp", "ep"),
            P("tp"),
            P(),
            P("ep", None, "tp", None),
            P("ep", None, "tp", None),
            P("ep"),
            P(),
            P("tp"),
            P("ep", None),
            P("ep", None),
            P("ep", "tp", None),
            P("ep", "tp", None),
            P("ep", None, "tp"),
            P("tp", "ep"),
            P("tp", "ep"),
            P("ep", "tp"),
            P(),
        ),
        out_specs=P("ep", "tp"),
        check_vma=False,
    )
```

time: 303 us -> 97.4 us (0.32)
  waiting for transfers between devices: 188 us -> 0 us
  Pallas kernels: 0 us -> 95.9 us
  starting transfers between devices: 34.8 us -> 0 us
  blocking collectives: 29.4 us -> 0 us
  matrix products: 14.9 us -> 0 us
  between operations: 13.9 us -> 0.01 us
  local copies, waits for them, and re-layouts: 11.5 us -> 1.3 us
  other arithmetic: 9.75 us -> 0 us
    psum x1 -> x0, waiting for transfers between devices: 109 us -> none  [packed_total(): so_far = lax.psum(jnp.concatenate([a.ravel() for a in arrays]), axis)]
    pallas_call x0 -> x1, Pallas kernels: none -> 95.9 us  [on_device(): pl.pallas_call(kernel, out_shape=jax.ShapeDtypeStruct((N, 256), BF16), in...]
    all_gather x1 -> x0, waiting for transfers between devices: 41.6 us -> none  [over_pieces(): return lax.all_gather(shard, axis).astype(jnp.float32).sum(0)]
    all_to_all x7 -> x0, waiting for transfers between devices: 36.9 us -> none  [the longest x2 6.87 us: sent_and_summed(): lax.all_to_all(tiles, axis, split_axis=0, concat_axis=0, tiled=True)]
    all_to_all x7 -> x0, starting transfers between devices: 34.7 us -> none  [the longest x1 7.57 us: on_device(): lax.all_to_all(tokens, 'ep', split_axis=1, concat_axis=0, tiled=True)]
    all_to_all x2 -> x0, blocking collectives: 29.4 us -> none  [sent_to_all(): return lax.all_to_all(copies, axis, split_axis=0, concat_axis=0, tiled=True)]
    dot_general x16 -> x0, matrix products: 14.9 us -> none  [the longest x1 3.04 us: attend(): jnp.einsum('skgcd,sjkcd->skgcj', query_rot, cached_keys, preferred_elemen...]
    unnamed x34 -> x1, local copies, waits for them, and re-layouts: 6.63 us -> 1.3 us
  transfers between devices with their start and end apart: 9 -> 0, of which waited for: 9 -> 0; matrix products, arithmetic and copies ran while one was open for 4% -> 0% of each run, Pallas kernels for 0% -> 0%
where the time goes in v1:
time: 97.4 us; the launch traced here: 97.2 us
  Pallas kernels  95.9 us (98%)
  local copies, waits for them, and re-layouts  1.3 us (1%)
    pallas_call x1, Pallas kernels, on_device(): pl.pallas_call(kernel, out_shape=jax.ShapeDtypeStruct((N, 256), BF16), in...  95.9 us

profile of v1, /device:TPU:1, one launch (start us, length us, event | category | flops | bytes accessed | tf_op | source)
XLA Modules:
  0.0 97.2 jit_solution(1430322677842592303)
XLA Ops:
  0.0 95.9 %layer.1 = bf16[16,256]{1,0:T(8,128)(2,1)} custom-call(bf16[16,4096]{1,0:T(8,128)(2,1)} %tok_h.1, bf16[256,256]{1,0:T(8,128)(2,1)} %qw_h.1, bf16[256,128]{1,0:T(8,128)(2,1)} %kw_h.1, bf16[256,128]{1,0:T(8,128)(2,1)} %vw_h.1, bf16[256,256]{1,0:T(8,128)(2,1)} %ow_h.1, f32[1,2]{1,0:T(1,128)} %bitcast.23, f32[1,128]{1,0:T(1,128)} %bitcast.24, ...), custom_call_target="tpu_custom_call" | custom-call | tf_op jit(solution)/shard_map/layer/pallas_call | solution.py:506
  95.9 1.3 %copy.23 = bf16[16,256]{1,0:T(8,128)(2,1)} copy(bf16[16,256]{1,0:T(8,128)(2,1)} %layer.1) | data formatting | bytes 16384

commit v2 on v1

v2 whole, which is shorter than its diff:
```python
import functools
import math

import jax
import jax.numpy as jnp
from jax import lax
from jax.experimental import pallas as pl
from jax.experimental.pallas import tpu as pltpu
from jax.sharding import PartitionSpec as P

N = 16
CACHE = 1024
CAP = 4
F32 = jnp.float32
BF16 = jnp.bfloat16
MESH = pl.DeviceIdType.MESH

(
    PA, PMETA, PB, PW1, PW2, PWGU, PWD, PE, PMEAN, PF, PG, PS, PX, PXR, PH, PI, PID, PC, PCD, PJ, PK,
) = range(21)
PHASES = 21

LOCALS = (
    "tok", "qw", "kw", "vw", "ow", "lam", "hgain", "kc", "vc", "lens", "fgain",
    "sgain", "ids", "rw", "eg", "eu", "ed", "dg", "du", "dd", "dmix",
)


def dot(a, b):
    return jnp.dot(a, b, preferred_element_type=F32)


def to_column(row, n):
    same = lax.broadcasted_iota(jnp.int32, (n, n), 0) == lax.broadcasted_iota(jnp.int32, (n, n), 1)
    return jnp.sum(jnp.where(same, jnp.broadcast_to(row, (n, n)), 0), axis=1, keepdims=True)


def to_row(column, n, lanes):
    same = lax.broadcasted_iota(jnp.int32, (n, lanes), 0) == lax.broadcasted_iota(
        jnp.int32, (n, lanes), 1
    )
    return jnp.sum(jnp.where(same, jnp.broadcast_to(column, (n, lanes)), 0), axis=0, keepdims=True)


def slot_of(i):
    return lax.rem(i, 2) * 8 + i // 2


def kernel(
    tok_h, qw_h, kw_h, vw_h, ow_h, lam_h, hgain_h, kc_h, vc_h, lens_h, fgain_h, sgain_h,
    ids_h, rw_h, eg_h, eu_h, ed_h, dg_h, du_h, dd_h, dmix_h,
    out_ref,
    tok, wqkv, wo, lam, hgain, kc, vc, lens, fgain, sgain, ids, rw, wgu, wgu2, ed, wd, wd2, dd, dmix,
    xcol, meta, metas, bsend, brecv, qs, kn, vn, h0, h1, lens_b, normed, esend, erecv,
    asend, arecv, fsend, frecv, gsend, grecv, ssend, srecv, gw, xsend, xrecv, xrows,
    hsend, hrecv, isend, idsend, ihid, idense,
    jsend, jrecv, ksend, krecv, pick, place, gates,
    lsem, ssem, rsem,
):
    e = lax.axis_index("ep")
    t = lax.axis_index("tp")
    z, c = t // 2, lax.rem(t, 2)
    partner = (e, 2 * z + 1 - c)
    y, x = e // 4, lax.rem(e, 4)
    e_slot = slot_of(e)

    def chunk(i, width):
        return pl.ds(pl.multiple_of(i * width, width), width)

    coming, flights = {}, []

    def bring(name, pairs, whole=None):
        sem = lsem.at[LOCALS.index(name)]
        coming[name] = pairs[0][1] if whole is None else whole
        for src, dst in pairs:
            pltpu.make_async_copy(src, dst, sem).start()

    def arrived(name):
        whole = coming.pop(name)
        pltpu.make_async_copy(whole, whole, lsem.at[LOCALS.index(name)]).wait()

    bring("tok", [(tok_h, tok)])
    bring("ids", [(ids_h, ids)])
    bring("rw", [(rw_h, rw)])
    bring("ow", [(ow_h, wo.at[y, x])])
    bring("qw", [(qw_h, wqkv.at[:, 0:256])])
    bring("kw", [(kw_h, wqkv.at[:, 256:384])])
    bring("vw", [(vw_h, wqkv.at[:, 384:512])])
    bring("lens", [(lens_h, lens)])
    bring("lam", [(lam_h, lam)])
    bring("hgain", [(hgain_h, hgain)])
    bring("fgain", [(fgain_h, fgain)])
    bring("dmix", [(dmix_h, dmix)])
    bring("sgain", [(sgain_h, sgain)])

    def bring_pair(i, _):
        sem_g = lsem.at[LOCALS.index("eg")]
        sem_u = lsem.at[LOCALS.index("eu")]
        core, chip = lax.rem(i, 2), i // 2
        even = pl.ds(pl.multiple_of(chip * 256, 256), 128)
        odd = pl.ds(pl.multiple_of(chip * 256 + 128, 128), 128)
        pltpu.make_async_copy(eg_h.at[:, chunk(i, 128)], wgu.at[core, :, even], sem_g).start()
        pltpu.make_async_copy(eu_h.at[:, chunk(i, 128)], wgu.at[core, :, odd], sem_u).start()
        return 0

    lax.fori_loop(0, N, bring_pair, 0)
    coming["eg"] = wgu.at[0]
    coming["eu"] = wgu.at[1]
    bring("dg", [(dg_h, wd.at[:, 0:128])])
    bring("du", [(du_h, wd.at[:, 128:256])])
    bring("kc", [(kc_h, kc)])
    bring("vc", [(vc_h, vc)])

    def bring_down(i, _):
        core, chip = lax.rem(i, 2), i // 2
        pltpu.make_async_copy(
            ed_h.at[chunk(i, 128), :], ed.at[core, chunk(chip, 128), :], lsem.at[LOCALS.index("ed")]
        ).start()
        return 0

    lax.fori_loop(0, N, bring_down, 0)
    coming["ed"] = ed
    bring("dd", [(dd_h, dd)])

    barrier = pltpu.get_barrier_semaphore()

    def greet(k, _):
        pl.semaphore_signal(
            barrier, inc=1, device_id=(lax.rem(e + k, N), t), device_id_type=MESH
        )
        pl.semaphore_signal(
            barrier, inc=1, device_id=(e, lax.rem(t + k, N)), device_id_type=MESH
        )
        return 0

    lax.fori_loop(1, N, greet, 0)

    def send(phase, src, dst, to):
        pltpu.make_async_remote_copy(
            src_ref=src,
            dst_ref=dst,
            send_sem=ssem.at[phase],
            recv_sem=rsem.at[phase],
            device_id=to,
            device_id_type=MESH,
        ).start()

    def over_ep(phase, src_of, dst):
        def one(k, _):
            a = lax.rem(e + k, N)
            send(phase, src_of(a), dst, (a, t))
            return 0

        lax.fori_loop(1, N, one, 0)

    def far_first(i, n):
        half = (i + 1) // 2
        return n // 2 + half * (2 * lax.rem(i + 1, 2) - 1)

    def over_tp(phase, src_of, dst):
        def one(i, _):
            b = lax.rem(t + far_first(i, N), N)
            send(phase, src_of(b), dst, (e, b))
            return 0

        lax.fori_loop(0, N - 1, one, 0)

    def over_z(phase, src_of, dst):
        def one(i, _):
            chip = lax.rem(z + far_first(i, 8), 8)
            send(phase, src_of(chip), dst, (e, 2 * chip + c))
            return 0

        lax.fori_loop(0, 7, one, 0)

    def received(phase, blocks):
        pltpu.make_async_copy(blocks, blocks, rsem.at[phase]).wait()

    def sent(phase, blocks):
        pltpu.make_async_copy(blocks, blocks, ssem.at[phase]).wait()

    lane = lax.broadcasted_iota(jnp.int32, (N, 128), 1)

    arrived("ids")
    arrived("rw")
    id0 = to_column(ids[0:1, :], N)
    id1 = to_column(ids[1:2, :], N)
    w0 = to_column(rw[0:1, :], N)
    w1 = to_column(rw[1:2, :], N)
    total = w0 + w1
    hit0 = lane == id0
    hit1 = lane == id1
    hit = jnp.where(hit0 | hit1, 1.0, 0.0).astype(F32)
    before = jnp.where(
        lax.broadcasted_iota(jnp.int32, (N, N), 1) < lax.broadcasted_iota(jnp.int32, (N, N), 0),
        1.0,
        0.0,
    ).astype(F32)
    slot = dot(before.astype(BF16), hit.astype(BF16))
    code = jnp.where(hit > 0.5, slot, -1.0)
    gate0 = jnp.where(lane - N == id0, w0 / total, 0.0)
    gate1 = jnp.where(lane - N == id1, w1 / total, 0.0)
    meta[...] = jnp.where(lane < N, code, gate0 + gate1)
    metas[e_slot] = meta[...]

    arrived("lens")
    length = to_column(lens[...], N)
    lens_b[...] = jnp.broadcast_to(length, (N, 128))
    turn = lax.rem(lane, 32).astype(F32) * (2.0 / 64)
    angle = length.astype(F32) * jnp.exp(turn * (-math.log(500000.0)))
    low = lax.rem(lane, 64) < 32
    cosine = jnp.cos(angle)
    sine = jnp.sin(angle)
    sine = jnp.where(low, -sine, sine)

    arrived("tok")
    xcol[e] = tok[:, chunk(e, 256)]
    arrived("ow")

    pl.semaphore_wait(barrier, 2 * (N - 1))

    over_ep(PA, lambda a: tok.at[:, chunk(a, 256)], xcol.at[e])
    flights.append((PA, xcol.at[0:15]))

    def first_half(k, _):
        send(PW1, wo.at[y, x, 0:128], wo.at[y, x, 0:128], (4 * y + lax.rem(x + k, 4), t))
        send(PW1, wo.at[y, x, 128:256], wo.at[y, x, 128:256], (4 * lax.rem(y + k, 4) + x, t))
        return 0

    lax.fori_loop(1, 4, first_half, 0)
    flights.append((PW1, wo.at[0, 0:3]))

    arrived("qw")
    arrived("kw")
    arrived("vw")
    received(PA, xcol.at[0:15])
    bsend[...] = dot(xcol[...].reshape(256, 256), wqkv[...]).astype(BF16).reshape(N, N, 512)
    brecv[e] = bsend[e]
    over_ep(PB, lambda a: bsend.at[a], brecv.at[e])
    flights.append((PB, bsend.at[0:15]))
    over_ep(PMETA, lambda a: meta, metas.at[e_slot])
    flights.append((PMETA, metas.at[0:15]))

    received(PW1, wo.at[0, 0:3])

    def second_half(k, _):
        send(PW2, wo.at[y, :, 0:128], wo.at[y, :, 0:128], (4 * lax.rem(y + k, 4) + x, t))
        send(PW2, wo.at[:, x, 128:256], wo.at[:, x, 128:256], (4 * y + lax.rem(x + k, 4), t))
        return 0

    lax.fori_loop(1, 4, second_half, 0)
    flights.append((PW2, wo.at[0:3]))

    arrived("eg")
    arrived("eu")
    arrived("dg")
    arrived("du")
    send(PWGU, wgu.at[1 - c], wgu2, partner)
    flights.append((PWGU, wgu2))
    send(PWD, wd, wd2, partner)
    flights.append((PWD, wd2))

    received(PB, brecv.at[0:15])
    qkv = jnp.sum(brecv[...].astype(F32), axis=0).astype(BF16).astype(F32)

    def rotated(v):
        swapped = jnp.where(low, pltpu.roll(v, 96, 1), pltpu.roll(v, 32, 1))
        return (v * cosine + swapped * sine).astype(BF16).astype(F32)

    first = lane < 64
    qs[...] = jnp.zeros_like(qs)
    for g in range(2):
        q = rotated(qkv[:, g * 128 : (g + 1) * 128]) * 0.125
        qs[pl.ds(g, N, stride=8), :] = jnp.where(first, q, 0.0)
        qs[pl.ds(g + 4, N, stride=8), :] = jnp.where(first, 0.0, q)
    kn[...] = rotated(qkv[:, 256:384])
    vn[...] = qkv[:, 384:512]

    arrived("lam")
    row8 = lax.broadcasted_iota(jnp.int32, (8, 1), 0)
    share = jnp.where(row8 == 4, -lam[0:1, 0:1], jnp.where(row8 == 5, -lam[0:1, 1:2], 1.0))
    place_of = lax.broadcasted_iota(jnp.int32, (8, CACHE), 1)

    arrived("kc")
    arrived("vc")

    def attend(s):
        q = qs[pl.ds(pl.multiple_of(s * 8, 8), 8), :]
        scores = lax.dot_general(
            q.astype(BF16), kc[s], (((1,), (1,)), ((), ())), preferred_element_type=F32
        )
        fresh = jnp.sum(q * kn[pl.ds(s, 1), :], axis=1, keepdims=True)
        scores = jnp.where(place_of < lens_b[pl.ds(s, 1), 0:1], scores, -1e30)
        top = jnp.maximum(jnp.max(scores, axis=1, keepdims=True), fresh)
        p = jnp.exp(scores - top)
        fresh_p = jnp.exp(fresh - top)
        scale = share / (jnp.sum(p, axis=1, keepdims=True) + fresh_p)
        p = p * scale
        fresh_p = fresh_p * scale
        p = p + pltpu.roll(p, 4, 0)
        fresh_p = jnp.broadcast_to(fresh_p, (8, 128))
        fresh_p = (fresh_p + pltpu.roll(fresh_p, 4, 0)).astype(BF16).astype(F32)
        head = dot(p.astype(BF16), vc[s]) + fresh_p * vn[pl.ds(s, 1), :]
        h0[pl.ds(s, 1), :] = head[0:1, :]
        h1[pl.ds(s, 1), :] = head[1:2, :]

    def attend_some(i, _):
        for j in range(4):
            attend(i * 4 + j)
        return 0

    lax.fori_loop(0, N // 4, attend_some, 0)

    arrived("hgain")
    for g, ref in enumerate((h0, h1)):
        head = ref[...]
        mean = jnp.mean(head * head, axis=1, keepdims=True)
        head = head * lax.rsqrt(mean + 1e-6) * hgain[...] * 0.8
        normed[:, g * 128 : (g + 1) * 128] = head.astype(BF16)
    received(PW2, wo.at[0:3])

    def out_block(b):
        part = dot(normed[...], wo[b // 4, lax.rem(b, 4)])
        esend[b] = part.astype(BF16)
        return part

    def out_send(i, sums):
        b = lax.rem(t + far_first(i, N), N)
        part = out_block(b)
        send(PE, esend.at[b], erecv.at[t], (e, b))
        return sums + part

    sums = lax.fori_loop(0, N - 1, out_send, jnp.zeros((N, 256), F32))
    flights.append((PE, esend.at[0:15]))
    sums = jnp.sum(sums + out_block(t), axis=1, keepdims=True)
    erecv[t] = esend[t]
    asend[...] = to_row(sums, N, 128)
    arecv[t] = asend[...]
    over_tp(PMEAN, lambda b: asend, arecv.at[t])
    flights.append((PMEAN, arecv.at[0:15]))

    received(PMETA, metas.at[0:15])
    every = metas[...].reshape(256, 128)
    wide_lane = lax.broadcasted_iota(jnp.int32, (256, 128), 1)
    code_col = jnp.sum(jnp.where(wide_lane == e, every, 0.0), axis=1, keepdims=True)
    gate_col = jnp.sum(jnp.where(wide_lane == e + N, every, 0.0), axis=1, keepdims=True)
    block = (lax.broadcasted_iota(jnp.int32, (256, 1), 0) // N * CAP).astype(F32)
    target = jnp.where(code_col >= 0.0, code_col + block, -1.0)
    place[...] = jnp.where(
        lax.broadcasted_iota(jnp.int32, (256, 64), 1).astype(F32) == target, 1.0, 0.0
    ).astype(BF16)
    pick[...] = jnp.where(
        lax.broadcasted_iota(jnp.int32, (64, 256), 0).astype(F32) == to_row(target, 256, 256),
        1.0,
        0.0,
    ).astype(BF16)
    gates[...] = gate_col

    arrived("fgain")
    arrived("dmix")
    gw[...] = fgain[...] * dmix[...].astype(F32)

    def block_of(ref):
        return jnp.concatenate([ref[pl.ds(2 * t, 1), :], ref[pl.ds(2 * t + 1, 1), :]], axis=1)

    gain = block_of(fgain)
    gain_mix = block_of(gw)
    root = 2.0**0.5
    token_mean = root * jnp.mean(tok[...].astype(F32), axis=1, keepdims=True)
    own_tokens = root * tok[:, chunk(t, 256)].astype(F32)

    received(PE, erecv.at[0:15])
    residual = own_tokens + jnp.sum(erecv[...].astype(F32), axis=0)
    received(PMEAN, arecv.at[0:15])
    mean = token_mean + to_column_of(jnp.sum(arecv[...], axis=0)) * (1.0 / 4096)
    centred = residual - mean
    gsend[...] = (centred * gain).astype(BF16)
    grecv[e_slot] = gsend[...]
    over_ep(PG, lambda a: gsend, grecv.at[e_slot])
    flights.append((PG, grecv.at[0:15]))
    fsend[0:1, :] = to_row(jnp.sum(centred * centred, axis=1, keepdims=True), N, 128)
    fsend[1:2, :] = to_row(jnp.sum(centred * gain_mix, axis=1, keepdims=True), N, 128)
    frecv[t] = fsend[...]
    over_tp(PF, lambda b: fsend, frecv.at[t])
    flights.append((PF, frecv.at[0:15]))

    received(PG, grecv.at[0:15])
    xsend[...] = dot(pick[...], grecv[...].reshape(256, 256)).astype(BF16)
    send(PX, xsend, xrecv, partner)
    flights.append((PX, xrecv))
    send(PXR, grecv.at[pl.ds((1 - c) * 8, 8)], xrows, partner)
    flights.append((PXR, xrows))

    received(PF, frecv.at[0:15])
    totals = jnp.sum(frecv[...], axis=0)
    scale_row = lax.rsqrt(totals[0:1, :] * (1.0 / 4096) + 1e-5)
    mix = 1.0 / (1.0 + jnp.exp(-scale_row * totals[1:2, :]))
    ssend[0:1, :] = scale_row
    ssend[1:2, :] = mix
    srecv[e_slot] = ssend[...]
    over_ep(PS, lambda a: ssend, srecv.at[e_slot])
    flights.append((PS, srecv.at[0:15]))

    received(PWGU, wgu2)
    received(PWD, wd2)
    received(PX, xrecv)
    received(PXR, xrows)
    mine = grecv[pl.ds(c * 8, 8)].reshape(128, 256)
    dense_pre = dot(mine, wd[...]) + dot(xrows[...].reshape(128, 256), wd2[...])
    hsend[:, 64:80, :] = dense_pre.astype(BF16).reshape(8, N, 256)

    def partial(chip):
        cols = chunk(chip, 256)
        pre = dot(xsend[...], wgu[c, :, cols]) + dot(xrecv[...], wgu2[:, cols])
        hsend[chip, 0:64, :] = pre.astype(BF16)

    def project(i, _):
        chip = lax.rem(z + far_first(i, 8), 8)
        partial(chip)
        send(PH, hsend.at[chip], hrecv.at[z], (e, 2 * chip + c))
        return 0

    lax.fori_loop(0, 7, project, 0)
    flights.append((PH, hsend.at[0:7]))
    partial(z)
    hrecv[z] = hsend[z]

    received(PS, srecv.at[0:15])
    own = lax.broadcasted_iota(jnp.int32, (N, N, 128), 1) == lax.broadcasted_iota(
        jnp.int32, (N, N, 128), 2
    )

    def token_column(rows):
        spread = jnp.where(own, jnp.broadcast_to(rows, (N, N, 128)), 0.0)
        return jnp.sum(spread, axis=2, keepdims=True).reshape(256, 1)

    mix_col = token_column(srecv[:, 1:2, :])
    scale_col = token_column(srecv[:, 0:1, :])
    row_scale = to_column(
        jnp.sum(jnp.where(place[...].astype(F32) > 0.5, scale_col, 0.0), axis=0, keepdims=True), 64
    )
    dense_scale = to_column_of(srecv[slot_of(t), 0:1, :])
    all_scale = jnp.concatenate([row_scale, dense_scale], axis=0)
    hidden = centred * to_column_of(scale_row) * gain

    received(PH, hrecv.at[0:7])
    pre = jnp.sum(hrecv[...].astype(F32), axis=0) * all_scale
    pre_gate = pre[:, 0:128]
    active = (pre_gate / (1.0 + jnp.exp(-pre_gate)) * pre[:, 128:256]).astype(BF16)
    isend[...] = active[0:64, :]
    idsend[...] = active[64:80, :]
    ihid[c, :, chunk(z, 128)] = isend[...]
    idense[c * 8 + z] = idsend[...]
    over_z(PI, lambda chip: isend, ihid.at[c, :, chunk(z, 128)])
    flights.append((PI, ihid.at[0, :, 0 : 7 * 128]))
    over_z(PID, lambda chip: idsend, idense.at[c * 8 + z])
    flights.append((PID, idense.at[0:7]))
    arrived("ed")
    arrived("dd")
    received(PI, ihid.at[0, :, 0 : 7 * 128])
    send(PC, ihid.at[c], ihid.at[c], partner)
    flights.append((PC, ihid.at[0]))
    received(PID, idense.at[0:7])
    send(PCD, idense.at[pl.ds(c * 8, 8)], idense.at[pl.ds(c * 8, 8)], partner)
    flights.append((PCD, idense.at[0:8]))
    result = dot(ihid[c], ed[c])
    received(PC, ihid.at[0])
    received(PCD, idense.at[0:8])
    result = (result + dot(ihid[1 - c], ed[1 - c])).astype(BF16)
    dense = dot(idense[...].reshape(256, 128), dd[...]) * mix_col
    mixture = dot(place[...], result) * gates[...] + dense
    jsend[...] = mixture.astype(BF16).reshape(N, N, 256)
    jrecv[e] = jsend[e_slot]
    over_ep(PJ, lambda a: jsend.at[slot_of(a)], jrecv.at[e])
    flights.append((PJ, jsend.at[0:15]))
    arrived("sgain")
    received(PJ, jrecv.at[0:15])
    combined = root * hidden.astype(BF16).astype(F32) + jnp.sum(jrecv[...].astype(F32), axis=0)

    mean_b = jnp.sum(combined, axis=1, keepdims=True) * (1.0 / 256)
    apart = combined - mean_b
    ksend[0:1, :] = to_row(mean_b, N, 128)
    ksend[1:2, :] = to_row(jnp.sum(apart * apart, axis=1, keepdims=True), N, 128)
    krecv[t] = ksend[...]
    over_tp(PK, lambda b: ksend, krecv.at[t])
    flights.append((PK, krecv.at[0:15]))
    received(PK, krecv.at[0:15])
    means = krecv[:, 0, :]
    mean = jnp.sum(means, axis=0, keepdims=True) * (1.0 / N)
    off = means - mean
    square = jnp.sum(krecv[:, 1, :] + 256.0 * off * off, axis=0, keepdims=True)
    scale = lax.rsqrt(square * (1.0 / 4096) + 1e-5)
    last_gain = jnp.concatenate([sgain[0:1, :], sgain[1:2, :]], axis=1)
    out_ref[...] = (
        (combined - to_column_of(mean)) * to_column_of(scale) * last_gain
    ).astype(BF16)

    for phase, blocks in flights:
        sent(phase, blocks)


def to_column_of(row):
    same = lax.broadcasted_iota(jnp.int32, (N, 128), 0) == lax.broadcasted_iota(
        jnp.int32, (N, 128), 1
    )
    return jnp.sum(jnp.where(same, jnp.broadcast_to(row, (N, 128)), 0), axis=1, keepdims=True)


def on_device(
    tokens, query_weight, key_weight, value_weight, out_weight, head_lambda, head_gain,
    key_cache, value_cache, lengths, first_gain, second_gain, expert_ids, route_weights,
    expert_gate, expert_up, expert_down, dense_gate, dense_up, dense_down, dense_mix,
):
    anywhere = pl.BlockSpec(memory_space=pltpu.HBM)
    vmem = pltpu.VMEM
    scratch = [
        vmem((N, 4096), BF16),
        vmem((256, 512), BF16),
        vmem((4, 4, 256, 256), BF16),
        vmem((1, 2), F32),
        vmem((1, 128), F32),
        vmem((N, CACHE, 128), BF16),
        vmem((N, CACHE, 128), BF16),
        vmem((1, N), jnp.int32),
        vmem((32, 128), F32),
        vmem((2, 128), F32),
        vmem((2, N), jnp.int32),
        vmem((2, N), F32),
        vmem((2, 256, 2048), BF16),
        vmem((256, 2048), BF16),
        vmem((2, 1024, 256), BF16),
        vmem((256, 256), BF16),
        vmem((256, 256), BF16),
        vmem((128, 256), BF16),
        vmem((32, 128), BF16),
        vmem((N, N, 256), BF16),
        vmem((N, 128), F32),
        vmem((N, N, 128), F32),
        vmem((N, N, 512), BF16),
        vmem((N, N, 512), BF16),
        vmem((128, 128), F32),
        vmem((N, 128), F32),
        vmem((N, 128), F32),
        vmem((N, 128), F32),
        vmem((N, 128), F32),
        vmem((N, 128), jnp.int32),
        vmem((N, 256), BF16),
        vmem((N, N, 256), BF16),
        vmem((N, N, 256), BF16),
        vmem((1, 128), F32),
        vmem((N, 1, 128), F32),
        vmem((2, 128), F32),
        vmem((N, 2, 128), F32),
        vmem((N, 256), BF16),
        vmem((N, N, 256), BF16),
        vmem((2, 128), F32),
        vmem((N, 2, 128), F32),
        vmem((32, 128), F32),
        vmem((64, 256), BF16),
        vmem((64, 256), BF16),
        vmem((8, N, 256), BF16),
        vmem((8, 80, 256), BF16),
        vmem((8, 80, 256), BF16),
        vmem((64, 128), BF16),
        vmem((N, 128), BF16),
        vmem((2, 64, 1024), BF16),
        vmem((N, N, 128), BF16),
        vmem((N, N, 256), BF16),
        vmem((N, N, 256), BF16),
        vmem((2, 128), F32),
        vmem((N, 2, 128), F32),
        vmem((64, 256), BF16),
        vmem((256, 64), BF16),
        vmem((256, 1), F32),
        pltpu.SemaphoreType.DMA((len(LOCALS),)),
        pltpu.SemaphoreType.DMA((PHASES,)),
        pltpu.SemaphoreType.DMA((PHASES,)),
    ]
    return pl.pallas_call(
        kernel,
        out_shape=jax.ShapeDtypeStruct((N, 256), BF16),
        in_specs=[anywhere] * 21,
        out_specs=pl.BlockSpec(memory_space=pltpu.VMEM),
        scratch_shapes=scratch,
        compiler_params=pltpu.CompilerParams(
            collective_id=0, has_side_effects=True, vmem_limit_bytes=67_043_328
        ),
        name="layer",
    )(
        tokens,
        query_weight,
        key_weight,
        value_weight,
        out_weight,
        head_lambda.reshape(1, 2),
        head_gain.reshape(1, 128),
        key_cache.reshape(N, CACHE, 128),
        value_cache.reshape(N, CACHE, 128),
        lengths.reshape(1, N),
        first_gain.reshape(32, 128),
        second_gain.reshape(2, 128),
        expert_ids.T,
        route_weights.T,
        expert_gate.reshape(256, 2048),
        expert_up.reshape(256, 2048),
        expert_down.reshape(2048, 256),
        dense_gate,
        dense_up,
        dense_down,
        dense_mix.reshape(32, 128),
    )


def solution(mesh):
    return jax.shard_map(
        on_device,
        mesh=mesh,
        in_specs=(
            P("ep", None),
            P("ep", "tp"),
            P("ep", "tp"),
            P("ep", "tp"),
            P("tp", "ep"),
            P("tp"),
            P(),
            P("ep", None, "tp", None),
            P("ep", None, "tp", None),
            P("ep"),
            P(),
            P("tp"),
            P("ep", None),
            P("ep", None),
            P("ep", "tp", None),
            P("ep", "tp", None),
            P("ep", None, "tp"),
            P("tp", "ep"),
            P("tp", "ep"),
            P("ep", "tp"),
            P(),
        ),
        out_specs=P("ep", "tp"),
        check_vma=False,
    )
```

time: 97.4 us -> 79.3 us (0.81)
  Pallas kernels: 95.9 us -> 77.8 us
    pallas_call x1, Pallas kernels: 95.9 us -> 77.8 us  [on_device(): pl.pallas_call(kernel, out_shape=jax.ShapeDtypeStruct((N, 256), BF16), in...]
where the time goes in v2:
time: 79.3 us; the launch traced here: 79.1 us
  Pallas kernels  77.8 us (98%)
  local copies, waits for them, and re-layouts  1.3 us (2%)
    pallas_call x1, Pallas kernels, on_device(): pl.pallas_call(kernel, out_shape=jax.ShapeDtypeStruct((N, 256), BF16), in...  77.8 us

profile of v2, /device:TPU:1, one launch (start us, length us, event | category | flops | bytes accessed | tf_op | source)
XLA Modules:
  0.0 79.1 jit_solution(18164317230128349912)
XLA Ops:
  0.0 77.8 %layer.1 = bf16[16,256]{1,0:T(8,128)(2,1)} custom-call(bf16[16,4096]{1,0:T(8,128)(2,1)} %tok_h.1, bf16[256,256]{1,0:T(8,128)(2,1)} %qw_h.1, bf16[256,128]{1,0:T(8,128)(2,1)} %kw_h.1, bf16[256,128]{1,0:T(8,128)(2,1)} %vw_h.1, bf16[256,256]{1,0:T(8,128)(2,1)} %ow_h.1, f32[1,2]{1,0:T(1,128)} %bitcast.23, f32[1,128]{1,0:T(1,128)} %bitcast.24, ...), custom_call_target="tpu_custom_call" | custom-call | tf_op jit(solution)/shard_map/layer/pallas_call | solution.py:579
  77.8 1.3 %copy.23 = bf16[16,256]{1,0:T(8,128)(2,1)} copy(bf16[16,256]{1,0:T(8,128)(2,1)} %layer.1) | data formatting | bytes 16384

commit v3 on v2

--- a/solution.py
+++ b/solution.py
@@ -16,9 +16,9 @@
 MESH = pl.DeviceIdType.MESH
 
 (
-    PA, PMETA, PB, PW1, PW2, PWGU, PWD, PE, PMEAN, PF, PG, PS, PX, PXR, PH, PI, PID, PC, PCD, PJ, PK,
-) = range(21)
-PHASES = 21
+    PA, PMETA, PB, PV, PW1, PW2, PWGU, PWD, PD, PE, PMEAN, PF, PG, PS, PX, PXR, PH, PI, PID, PC, PCD, PJ, PK,
+) = range(23)
+PHASES = 23
 
 LOCALS = (
     "tok", "qw", "kw", "vw", "ow", "lam", "hgain", "kc", "vc", "lens", "fgain",
@@ -51,11 +51,11 @@
     ids_h, rw_h, eg_h, eu_h, ed_h, dg_h, du_h, dd_h, dmix_h,
     out_ref,
     tok, wqkv, wo, lam, hgain, kc, vc, lens, fgain, sgain, ids, rw, wgu, wgu2, ed, wd, wd2, dd, dmix,
-    xcol, meta, metas, bsend, brecv, qs, kn, vn, h0, h1, lens_b, normed, esend, erecv,
+    xcol, meta, metas, bsend, brecv, qd, scores, normed, dnorm, vsend, vrecv, esend, erecv,
     asend, arecv, fsend, frecv, gsend, grecv, ssend, srecv, gw, xsend, xrecv, xrows,
     hsend, hrecv, isend, idsend, ihid, idense,
     jsend, jrecv, ksend, krecv, pick, place, gates,
-    lsem, ssem, rsem,
+    lsem, ssem, rsem, ready,
 ):
     e = lax.axis_index("ep")
     t = lax.axis_index("tp")
@@ -67,6 +67,19 @@
     def chunk(i, width):
         return pl.ds(pl.multiple_of(i * width, width), width)
 
+    barrier = pltpu.get_barrier_semaphore()
+
+    def greet(k, _):
+        pl.semaphore_signal(
+            barrier, inc=1, device_id=(lax.rem(e + k, N), t), device_id_type=MESH
+        )
+        pl.semaphore_signal(
+            barrier, inc=1, device_id=(e, lax.rem(t + k, N)), device_id_type=MESH
+        )
+        return 0
+
+    lax.fori_loop(1, N, greet, 0)
+
     coming, flights = {}, []
 
     def bring(name, pairs, whole=None):
@@ -82,7 +95,7 @@
     bring("tok", [(tok_h, tok)])
     bring("ids", [(ids_h, ids)])
     bring("rw", [(rw_h, rw)])
-    bring("ow", [(ow_h, wo.at[y, x])])
+    bring("ow", [(ow_h, wo.at[x])])
     bring("qw", [(qw_h, wqkv.at[:, 0:256])])
     bring("kw", [(kw_h, wqkv.at[:, 256:384])])
     bring("vw", [(vw_h, wqkv.at[:, 384:512])])
@@ -108,8 +121,8 @@
     coming["eu"] = wgu.at[1]
     bring("dg", [(dg_h, wd.at[:, 0:128])])
     bring("du", [(du_h, wd.at[:, 128:256])])
-    bring("kc", [(kc_h, kc)])
-    bring("vc", [(vc_h, vc)])
+    bring("kc", [(kc_h.at[s], kc.at[:, s * 128 : (s + 1) * 128]) for s in range(N)], kc)
+    bring("vc", [(vc_h.at[s], vc.at[:, s * 128 : (s + 1) * 128]) for s in range(N)], vc)
 
     def bring_down(i, _):
         core, chip = lax.rem(i, 2), i // 2
@@ -121,19 +134,6 @@
     lax.fori_loop(0, N, bring_down, 0)
     coming["ed"] = ed
     bring("dd", [(dd_h, dd)])
-
-    barrier = pltpu.get_barrier_semaphore()
-
-    def greet(k, _):
-        pl.semaphore_signal(
-            barrier, inc=1, device_id=(lax.rem(e + k, N), t), device_id_type=MESH
-        )
-        pl.semaphore_signal(
-            barrier, inc=1, device_id=(e, lax.rem(t + k, N)), device_id_type=MESH
-        )
-        return 0
-
-    lax.fori_loop(1, N, greet, 0)
 
     def send(phase, src, dst, to):
         pltpu.make_async_remote_copy(
@@ -205,7 +205,6 @@
 
     arrived("lens")
     length = to_column(lens[...], N)
-    lens_b[...] = jnp.broadcast_to(length, (N, 128))
     turn = lax.rem(lane, 32).astype(F32) * (2.0 / 64)
     angle = length.astype(F32) * jnp.exp(turn * (-math.log(500000.0)))
     low = lax.rem(lane, 64) < 32
@@ -216,19 +215,28 @@
     arrived("tok")
     xcol[e] = tok[:, chunk(e, 256)]
     arrived("ow")
+    heads_sum = to_row(jnp.sum(wo[x].astype(F32), axis=1, keepdims=True), 256, 256)
+    vsend[0:1, :] = heads_sum[:, 0:128]
+    vsend[1:2, :] = heads_sum[:, 128:256]
+    vrecv[e] = vsend[...]
 
     pl.semaphore_wait(barrier, 2 * (N - 1))
 
     over_ep(PA, lambda a: tok.at[:, chunk(a, 256)], xcol.at[e])
     flights.append((PA, xcol.at[0:15]))
 
-    def first_half(k, _):
-        send(PW1, wo.at[y, x, 0:128], wo.at[y, x, 0:128], (4 * y + lax.rem(x + k, 4), t))
-        send(PW1, wo.at[y, x, 128:256], wo.at[y, x, 128:256], (4 * lax.rem(y + k, 4) + x, t))
+    after, ahead = 4 * y + lax.rem(x + 1, 4), 4 * y + lax.rem(x + 3, 4)
+    send(PW1, wo.at[x], wo.at[x], (after, t))
+    send(PW1, wo.at[x], wo.at[x], (ahead, t))
+    flights.append((PW1, wo.at[0:2]))
+    over_ep(PV, lambda a: vsend, vrecv.at[e])
+    flights.append((PV, vrecv.at[0:15]))
+
+    def tell(k, _):
+        pl.semaphore_signal(ready, inc=1, device_id=(e, lax.rem(t + k, N)), device_id_type=MESH)
         return 0
 
-    lax.fori_loop(1, 4, first_half, 0)
-    flights.append((PW1, wo.at[0, 0:3]))
+    lax.fori_loop(1, N, tell, 0)
 
     arrived("qw")
     arrived("kw")
@@ -238,18 +246,12 @@
     brecv[e] = bsend[e]
     over_ep(PB, lambda a: bsend.at[a], brecv.at[e])
     flights.append((PB, bsend.at[0:15]))
-    over_ep(PMETA, lambda a: meta, metas.at[e_slot])
-    flights.append((PMETA, metas.at[0:15]))
-
-    received(PW1, wo.at[0, 0:3])
-
-    def second_half(k, _):
-        send(PW2, wo.at[y, :, 0:128], wo.at[y, :, 0:128], (4 * lax.rem(y + k, 4) + x, t))
-        send(PW2, wo.at[:, x, 128:256], wo.at[:, x, 128:256], (4 * y + lax.rem(x + k, 4), t))
-        return 0
-
-    lax.fori_loop(1, 4, second_half, 0)
-    flights.append((PW2, wo.at[0:3]))
+
+    received(PW1, wo.at[0:2])
+    x_up, x_down = lax.rem(x + 3, 4), lax.rem(x + 1, 4)
+    send(PW2, wo.at[x_up, 0:128], wo.at[x_up, 0:128], (after, t))
+    send(PW2, wo.at[x_down, 128:256], wo.at[x_down, 128:256], (ahead, t))
+    flights.append((PW2, wo.at[0]))
 
     arrived("eg")
     arrived("eu")
@@ -268,76 +270,107 @@
         return (v * cosine + swapped * sine).astype(BF16).astype(F32)
 
     first = lane < 64
-    qs[...] = jnp.zeros_like(qs)
+    key = rotated(qkv[:, 256:384])
+    value = qkv[:, 384:512]
+    parts, fresh = [], jnp.zeros((1, 128), F32)
+    seq = lax.broadcasted_iota(jnp.int32, (N, 128), 0)
+    for sub in range(2):
+        for g in range(2):
+            q = rotated(qkv[:, g * 128 : (g + 1) * 128]) * 0.125
+            q = jnp.where(first if sub == 0 else jnp.logical_not(first), q, 0.0)
+            score = jnp.sum(q * key, axis=1, keepdims=True)
+            at = lane == (2 * sub + g) * N + seq
+            fresh = fresh + jnp.sum(jnp.where(at, score, 0.0), axis=0, keepdims=True)
+            parts.append(q)
+    turned = jnp.concatenate(parts + [jnp.zeros((64, 128), F32)], axis=0).T
+    lane128 = lax.broadcasted_iota(jnp.int32, (128, 128), 1)
+    for s in range(N):
+        keep = (lax.rem(lane128, N) == s) & (lane128 < 64)
+        qd[s * 128 : (s + 1) * 128, :] = jnp.where(keep, turned, 0.0).astype(BF16)
+
+    arrived("lam")
+    row = lax.broadcasted_iota(jnp.int32, (1, 128), 1)
+    share = jnp.where(
+        row < 2 * N, 1.0, jnp.where(row < 3 * N, -lam[0:1, 0:1], -lam[0:1, 1:2])
+    )
+    limit = jnp.sum(jnp.where(lax.rem(lane, N) == seq, length, 0), axis=0, keepdims=True)
+
+    arrived("kc")
+    scores[...] = dot(kc[...], qd[...])
+    position = lax.broadcasted_iota(jnp.int32, (CACHE, 128), 0)
+    masked = jnp.where(position < limit, scores[...], -1e30)
+    top = jnp.maximum(jnp.max(masked, axis=0, keepdims=True), fresh)
+    p = jnp.exp(masked - top)
+    fresh_p = jnp.exp(fresh - top)
+    scale = share / (jnp.sum(p, axis=0, keepdims=True) + fresh_p)
+    p = p * scale
+    fresh_p = fresh_p * scale
+    p = p + pltpu.roll(p, 96, 1)
+    fresh_p = jnp.broadcast_to(fresh_p, (8, 128))
+    fresh_p = (fresh_p + pltpu.roll(fresh_p, 96, 1)).astype(BF16).astype(F32)[0:1, :]
+    chances = p.T[0 : 2 * N, :].astype(BF16)
+    arrived("vc")
+    heads = dot(chances, vc[...])
+
+    arrived("hgain")
     for g in range(2):
-        q = rotated(qkv[:, g * 128 : (g + 1) * 128]) * 0.125
-        qs[pl.ds(g, N, stride=8), :] = jnp.where(first, q, 0.0)
-        qs[pl.ds(g + 4, N, stride=8), :] = jnp.where(first, 0.0, q)
-    kn[...] = rotated(qkv[:, 256:384])
-    vn[...] = qkv[:, 384:512]
-
-    arrived("lam")
-    row8 = lax.broadcasted_iota(jnp.int32, (8, 1), 0)
-    share = jnp.where(row8 == 4, -lam[0:1, 0:1], jnp.where(row8 == 5, -lam[0:1, 1:2], 1.0))
-    place_of = lax.broadcasted_iota(jnp.int32, (8, CACHE), 1)
-
-    arrived("kc")
-    arrived("vc")
-
-    def attend(s):
-        q = qs[pl.ds(pl.multiple_of(s * 8, 8), 8), :]
-        scores = lax.dot_general(
-            q.astype(BF16), kc[s], (((1,), (1,)), ((), ())), preferred_element_type=F32
-        )
-        fresh = jnp.sum(q * kn[pl.ds(s, 1), :], axis=1, keepdims=True)
-        scores = jnp.where(place_of < lens_b[pl.ds(s, 1), 0:1], scores, -1e30)
-        top = jnp.maximum(jnp.max(scores, axis=1, keepdims=True), fresh)
-        p = jnp.exp(scores - top)
-        fresh_p = jnp.exp(fresh - top)
-        scale = share / (jnp.sum(p, axis=1, keepdims=True) + fresh_p)
-        p = p * scale
-        fresh_p = fresh_p * scale
-        p = p + pltpu.roll(p, 4, 0)
-        fresh_p = jnp.broadcast_to(fresh_p, (8, 128))
-        fresh_p = (fresh_p + pltpu.roll(fresh_p, 4, 0)).astype(BF16).astype(F32)
-        head = dot(p.astype(BF16), vc[s]) + fresh_p * vn[pl.ds(s, 1), :]
-        h0[pl.ds(s, 1), :] = head[0:1, :]
-        h1[pl.ds(s, 1), :] = head[1:2, :]
-
-    def attend_some(i, _):
-        for j in range(4):
-            attend(i * 4 + j)
-        return 0
-
-    lax.fori_loop(0, N // 4, attend_some, 0)
-
-    arrived("hgain")
-    for g, ref in enumerate((h0, h1)):
-        head = ref[...]
+        weight = jnp.sum(jnp.where(lane == g * N + seq, fresh_p, 0.0), axis=1, keepdims=True)
+        head = weight * value
+        for s in range(N):
+            head = head + jnp.where(
+                seq == s, heads[g * N : (g + 1) * N, s * 128 : (s + 1) * 128], 0.0
+            )
         mean = jnp.mean(head * head, axis=1, keepdims=True)
         head = head * lax.rsqrt(mean + 1e-6) * hgain[...] * 0.8
         normed[:, g * 128 : (g + 1) * 128] = head.astype(BF16)
-    received(PW2, wo.at[0:3])
-
-    def out_block(b):
-        part = dot(normed[...], wo[b // 4, lax.rem(b, 4)])
-        esend[b] = part.astype(BF16)
-        return part
-
-    def out_send(i, sums):
-        b = lax.rem(t + far_first(i, N), N)
-        part = out_block(b)
-        send(PE, esend.at[b], erecv.at[t], (e, b))
-        return sums + part
-
-    sums = lax.fori_loop(0, N - 1, out_send, jnp.zeros((N, 256), F32))
-    flights.append((PE, esend.at[0:15]))
-    sums = jnp.sum(sums + out_block(t), axis=1, keepdims=True)
-    erecv[t] = esend[t]
+    dnorm[y] = normed[...]
+
+    def heads_send(k, _):
+        send(PD, normed, dnorm.at[y], (4 * lax.rem(y + k, 4) + x, t))
+        return 0
+
+    lax.fori_loop(1, 4, heads_send, 0)
+    flights.append((PD, dnorm.at[0:3]))
+    received(PV, vrecv.at[0:15])
+    weights_sum = jnp.sum(vrecv[...], axis=0)
+    sums = jnp.sum(
+        normed[:, 0:128].astype(F32) * weights_sum[0:1, :]
+        + normed[:, 128:256].astype(F32) * weights_sum[1:2, :],
+        axis=1,
+        keepdims=True,
+    )
     asend[...] = to_row(sums, N, 128)
     arecv[t] = asend[...]
     over_tp(PMEAN, lambda b: asend, arecv.at[t])
     flights.append((PMEAN, arecv.at[0:15]))
+    pl.semaphore_wait(ready, N - 1)
+    received(PW2, wo.at[0])
+    received(PD, dnorm.at[0:3])
+
+    def out_send(i, _):
+        x2, y2 = i // 4, lax.rem(y + 2 + lax.rem(i, 4), 4)
+        b = 4 * y + x2
+        itself = (y2 == y) & (b == t)
+
+        @pl.when(lax.rem(i, 4) == 0)
+        def _():
+            part = dot(dnorm[...].reshape(64, 256), wo[x2])
+            esend[x2] = part.astype(BF16).reshape(4, N, 256)
+
+        @pl.when(itself)
+        def _():
+            pltpu.make_async_copy(esend.at[x2, y2], erecv.at[t], rsem.at[PE]).start()
+
+        @pl.when(jnp.logical_not(itself))
+        def _():
+            send(PE, esend.at[x2, y2], erecv.at[t], (4 * y2 + x, b))
+
+        return 0
+
+    lax.fori_loop(0, N, out_send, 0)
+    flights.append((PE, erecv.at[0:15]))
+    over_ep(PMETA, lambda a: meta, metas.at[e_slot])
+    flights.append((PMETA, metas.at[0:15]))
 
     received(PMETA, metas.at[0:15])
     every = metas[...].reshape(256, 128)
@@ -369,7 +402,7 @@
     token_mean = root * jnp.mean(tok[...].astype(F32), axis=1, keepdims=True)
     own_tokens = root * tok[:, chunk(t, 256)].astype(F32)
 
-    received(PE, erecv.at[0:15])
+    received(PE, erecv)
     residual = own_tokens + jnp.sum(erecv[...].astype(F32), axis=0)
     received(PMEAN, arecv.at[0:15])
     mean = token_mean + to_column_of(jnp.sum(arecv[...], axis=0)) * (1.0 / 4096)
@@ -391,6 +424,30 @@
     send(PXR, grecv.at[pl.ds((1 - c) * 8, 8)], xrows, partner)
     flights.append((PXR, xrows))
 
+    received(PWGU, wgu2)
+    received(PWD, wd2)
+    received(PX, xrecv)
+    received(PXR, xrows)
+    mine = grecv[pl.ds(c * 8, 8)].reshape(128, 256)
+    dense_pre = dot(mine, wd[...]) + dot(xrows[...].reshape(128, 256), wd2[...])
+    hsend[:, 64:80, :] = dense_pre.astype(BF16).reshape(8, N, 256)
+
+    def partial(chip):
+        cols = chunk(chip, 256)
+        pre = dot(xsend[...], wgu[c, :, cols]) + dot(xrecv[...], wgu2[:, cols])
+        hsend[chip, 0:64, :] = pre.astype(BF16)
+
+    def project(i, _):
+        chip = lax.rem(z + far_first(i, 8), 8)
+        partial(chip)
+        send(PH, hsend.at[chip], hrecv.at[z], (e, 2 * chip + c))
+        return 0
+
+    lax.fori_loop(0, 7, project, 0)
+    flights.append((PH, hsend.at[0:7]))
+    partial(z)
+    hrecv[z] = hsend[z]
+
     received(PF, frecv.at[0:15])
     totals = jnp.sum(frecv[...], axis=0)
     scale_row = lax.rsqrt(totals[0:1, :] * (1.0 / 4096) + 1e-5)
@@ -400,30 +457,6 @@
     srecv[e_slot] = ssend[...]
     over_ep(PS, lambda a: ssend, srecv.at[e_slot])
     flights.append((PS, srecv.at[0:15]))
-
-    received(PWGU, wgu2)
-    received(PWD, wd2)
-    received(PX, xrecv)
-    received(PXR, xrows)
-    mine = grecv[pl.ds(c * 8, 8)].reshape(128, 256)
-    dense_pre = dot(mine, wd[...]) + dot(xrows[...].reshape(128, 256), wd2[...])
-    hsend[:, 64:80, :] = dense_pre.astype(BF16).reshape(8, N, 256)
-
-    def partial(chip):
-        cols = chunk(chip, 256)
-        pre = dot(xsend[...], wgu[c, :, cols]) + dot(xrecv[...], wgu2[:, cols])
-        hsend[chip, 0:64, :] = pre.astype(BF16)
-
-    def project(i, _):
-        chip = lax.rem(z + far_first(i, 8), 8)
-        partial(chip)
-        send(PH, hsend.at[chip], hrecv.at[z], (e, 2 * chip + c))
-        return 0
-
-    lax.fori_loop(0, 7, project, 0)
-    flights.append((PH, hsend.at[0:7]))
-    partial(z)
-    hrecv[z] = hsend[z]
 
     received(PS, srecv.at[0:15])
     own = lax.broadcasted_iota(jnp.int32, (N, N, 128), 1) == lax.broadcasted_iota(
@@ -498,6 +531,12 @@
     for phase, blocks in flights:
         sent(phase, blocks)
 
+    if any(phase == PE for phase, _ in flights):
+
+        @pl.when(t // 4 != y)
+        def _():
+            sent(PE, erecv.at[0])
+
 
 def to_column_of(row):
     same = lax.broadcasted_iota(jnp.int32, (N, 128), 0) == lax.broadcasted_iota(
@@ -516,11 +555,11 @@
     scratch = [
         vmem((N, 4096), BF16),
         vmem((256, 512), BF16),
-        vmem((4, 4, 256, 256), BF16),
+        vmem((4, 256, 256), BF16),
         vmem((1, 2), F32),
         vmem((1, 128), F32),
-        vmem((N, CACHE, 128), BF16),
-        vmem((N, CACHE, 128), BF16),
+        vmem((CACHE, N * 128), BF16),
+        vmem((CACHE, N * 128), BF16),
         vmem((1, N), jnp.int32),
         vmem((32, 128), F32),
         vmem((2, 128), F32),
@@ -538,14 +577,13 @@
         vmem((N, N, 128), F32),
         vmem((N, N, 512), BF16),
         vmem((N, N, 512), BF16),
-        vmem((128, 128), F32),
-        vmem((N, 128), F32),
-        vmem((N, 128), F32),
-        vmem((N, 128), F32),
-        vmem((N, 128), F32),
-        vmem((N, 128), jnp.int32),
+        vmem((N * 128, 128), BF16),
+        vmem((CACHE, 128), F32),
         vmem((N, 256), BF16),
-        vmem((N, N, 256), BF16),
+        vmem((4, N, 256), BF16),
+        vmem((2, 128), F32),
+        vmem((N, 2, 128), F32),
+        vmem((4, 4, N, 256), BF16),
         vmem((N, N, 256), BF16),
         vmem((1, 128), F32),
         vmem((N, 1, 128), F32),
@@ -575,6 +613,7 @@
         pltpu.SemaphoreType.DMA((len(LOCALS),)),
         pltpu.SemaphoreType.DMA((PHASES,)),
         pltpu.SemaphoreType.DMA((PHASES,)),
+        pltpu.SemaphoreType.REGULAR,
     ]
     return pl.pallas_call(
         kernel,

time: 79.3 us -> 75.2 us (0.948)
  Pallas kernels: 77.8 us -> 73.8 us
    pallas_call x1, Pallas kernels: 77.8 us -> 73.8 us  [on_device(): pl.pallas_call(kernel, out_shape=jax.ShapeDtypeStruct((N, 256), BF16), in...]
where the time goes in v3:
time: 75.2 us; the launch traced here: 75.1 us
  Pallas kernels  73.8 us (98%)
  local copies, waits for them, and re-layouts  1.3 us (2%)
    pallas_call x1, Pallas kernels, on_device(): pl.pallas_call(kernel, out_shape=jax.ShapeDtypeStruct((N, 256), BF16), in...  73.8 us

profile of v3, /device:TPU:1, one launch (start us, length us, event | category | flops | bytes accessed | tf_op | source)
XLA Modules:
  0.0 75.1 jit_solution(13112460518561396912)
XLA Ops:
  0.0 73.8 %layer.1 = bf16[16,256]{1,0:T(8,128)(2,1)} custom-call(bf16[16,4096]{1,0:T(8,128)(2,1)} %tok_h.1, bf16[256,256]{1,0:T(8,128)(2,1)} %qw_h.1, bf16[256,128]{1,0:T(8,128)(2,1)} %kw_h.1, bf16[256,128]{1,0:T(8,128)(2,1)} %vw_h.1, bf16[256,256]{1,0:T(8,128)(2,1)} %ow_h.1, f32[1,2]{1,0:T(1,128)} %bitcast.23, f32[1,128]{1,0:T(1,128)} %bitcast.24, ...), custom_call_target="tpu_custom_call" | custom-call | tf_op jit(solution)/shard_map/layer/pallas_call | solution.py:618
  73.8 1.3 %copy.23 = bf16[16,256]{1,0:T(8,128)(2,1)} copy(bf16[16,256]{1,0:T(8,128)(2,1)} %layer.1) | data formatting | bytes 16384

commit v4 on v3

--- a/solution.py
+++ b/solution.py
@@ -50,7 +50,7 @@
     tok_h, qw_h, kw_h, vw_h, ow_h, lam_h, hgain_h, kc_h, vc_h, lens_h, fgain_h, sgain_h,
     ids_h, rw_h, eg_h, eu_h, ed_h, dg_h, du_h, dd_h, dmix_h,
     out_ref,
-    tok, wqkv, wo, lam, hgain, kc, vc, lens, fgain, sgain, ids, rw, wgu, wgu2, ed, wd, wd2, dd, dmix,
+    tok, wqkv, wown, wo, lam, hgain, kc, vc, lens, fgain, sgain, ids, rw, wgu, wgu2, ed, wd, wd2, dd, dmix,
     xcol, meta, metas, bsend, brecv, qd, scores, normed, dnorm, vsend, vrecv, esend, erecv,
     asend, arecv, fsend, frecv, gsend, grecv, ssend, srecv, gw, xsend, xrecv, xrows,
     hsend, hrecv, isend, idsend, ihid, idense,
@@ -95,7 +95,7 @@
     bring("tok", [(tok_h, tok)])
     bring("ids", [(ids_h, ids)])
     bring("rw", [(rw_h, rw)])
-    bring("ow", [(ow_h, wo.at[x])])
+    bring("ow", [(ow_h, wown)])
     bring("qw", [(qw_h, wqkv.at[:, 0:256])])
     bring("kw", [(kw_h, wqkv.at[:, 256:384])])
     bring("vw", [(vw_h, wqkv.at[:, 384:512])])
@@ -215,7 +215,7 @@
     arrived("tok")
     xcol[e] = tok[:, chunk(e, 256)]
     arrived("ow")
-    heads_sum = to_row(jnp.sum(wo[x].astype(F32), axis=1, keepdims=True), 256, 256)
+    heads_sum = to_row(jnp.sum(wown[...].astype(F32), axis=1, keepdims=True), 256, 256)
     vsend[0:1, :] = heads_sum[:, 0:128]
     vsend[1:2, :] = heads_sum[:, 128:256]
     vrecv[e] = vsend[...]
@@ -224,13 +224,6 @@
 
     over_ep(PA, lambda a: tok.at[:, chunk(a, 256)], xcol.at[e])
     flights.append((PA, xcol.at[0:15]))
-
-    after, ahead = 4 * y + lax.rem(x + 1, 4), 4 * y + lax.rem(x + 3, 4)
-    send(PW1, wo.at[x], wo.at[x], (after, t))
-    send(PW1, wo.at[x], wo.at[x], (ahead, t))
-    flights.append((PW1, wo.at[0:2]))
-    over_ep(PV, lambda a: vsend, vrecv.at[e])
-    flights.append((PV, vrecv.at[0:15]))
 
     def tell(k, _):
         pl.semaphore_signal(ready, inc=1, device_id=(e, lax.rem(t + k, N)), device_id_type=MESH)
@@ -247,11 +240,25 @@
     over_ep(PB, lambda a: bsend.at[a], brecv.at[e])
     flights.append((PB, bsend.at[0:15]))
 
-    received(PW1, wo.at[0:2])
-    x_up, x_down = lax.rem(x + 3, 4), lax.rem(x + 1, 4)
-    send(PW2, wo.at[x_up, 0:128], wo.at[x_up, 0:128], (after, t))
-    send(PW2, wo.at[x_down, 128:256], wo.at[x_down, 128:256], (ahead, t))
-    flights.append((PW2, wo.at[0]))
+    after, ahead = 4 * y + lax.rem(x + 1, 4), 4 * y + lax.rem(x + 3, 4)
+    goal = lax.rem(x, 2)
+    same = goal == c
+    other = jnp.logical_not(same)
+    landing = wo.at[x // 2, chunk(c, 256)]
+    send(PW1, wown, landing, (after, 2 * z + goal))
+    send(PW1, wown, landing, (ahead, 2 * z + goal))
+
+    @pl.when(same)
+    def _():
+        pltpu.make_async_copy(wown, landing, rsem.at[PW1]).start()
+
+    @pl.when(other)
+    def _():
+        send(PW1, wown, landing, partner)
+
+    flights.append((PW1, wo.at[0]))
+    over_ep(PV, lambda a: vsend, vrecv.at[e])
+    flights.append((PV, vrecv.at[0:15]))
 
     arrived("eg")
     arrived("eu")
@@ -310,6 +317,18 @@
     fresh_p = (fresh_p + pltpu.roll(fresh_p, 96, 1)).astype(BF16).astype(F32)[0:1, :]
     chances = p.T[0 : 2 * N, :].astype(BF16)
     arrived("vc")
+    @pl.when(same)
+    def _():
+        received(PW1, wo.at[0])
+
+    @pl.when(other)
+    def _():
+        received(PW1, wo)
+        x_up, x_down = lax.rem(x + 3, 4), lax.rem(x + 1, 4)
+        low_half, high_half = wo.at[x_down // 2, 0:256], wo.at[x_up // 2, 256:512]
+        send(PW2, low_half, low_half, (ahead, t))
+        send(PW2, high_half, high_half, (after, t))
+
     heads = dot(chances, vc[...])
 
     arrived("hgain")
@@ -323,14 +342,18 @@
         mean = jnp.mean(head * head, axis=1, keepdims=True)
         head = head * lax.rsqrt(mean + 1e-6) * hgain[...] * 0.8
         normed[:, g * 128 : (g + 1) * 128] = head.astype(BF16)
-    dnorm[y] = normed[...]
+    pl.semaphore_wait(ready, N - 1)
+    dnorm[c * 4 + y] = normed[...]
 
     def heads_send(k, _):
-        send(PD, normed, dnorm.at[y], (4 * lax.rem(y + k, 4) + x, t))
+        e2 = 4 * lax.rem(y + k, 4) + x
+        send(PD, normed, dnorm.at[c * 4 + y], (e2, t))
+        send(PD, normed, dnorm.at[c * 4 + y], (e2, 2 * z + 1 - c))
         return 0
 
     lax.fori_loop(1, 4, heads_send, 0)
-    flights.append((PD, dnorm.at[0:3]))
+    send(PD, normed, dnorm.at[c * 4 + y], partner)
+    flights.append((PD, dnorm.at[0:7]))
     received(PV, vrecv.at[0:15])
     weights_sum = jnp.sum(vrecv[...], axis=0)
     sums = jnp.sum(
@@ -343,32 +366,36 @@
     arecv[t] = asend[...]
     over_tp(PMEAN, lambda b: asend, arecv.at[t])
     flights.append((PMEAN, arecv.at[0:15]))
-    pl.semaphore_wait(ready, N - 1)
-    received(PW2, wo.at[0])
-    received(PD, dnorm.at[0:3])
+
+    @pl.when(same)
+    def _():
+        received(PW2, wo.at[0])
+
+    received(PD, dnorm.at[0:7])
 
     def out_send(i, _):
-        x2, y2 = i // 4, lax.rem(y + 2 + lax.rem(i, 4), 4)
-        b = 4 * y + x2
+        j, y2 = i // 4, lax.rem(y + 2 + lax.rem(i, 4), 4)
+        b = 4 * y + 2 * j + c
         itself = (y2 == y) & (b == t)
 
         @pl.when(lax.rem(i, 4) == 0)
         def _():
-            part = dot(dnorm[...].reshape(64, 256), wo[x2])
-            esend[x2] = part.astype(BF16).reshape(4, N, 256)
+            part = dot(dnorm[0:4].reshape(64, 256), wo[j, 0:256])
+            part = part + dot(dnorm[4:8].reshape(64, 256), wo[j, 256:512])
+            esend[j] = part.astype(BF16).reshape(4, N, 256)
 
         @pl.when(itself)
         def _():
-            pltpu.make_async_copy(esend.at[x2, y2], erecv.at[t], rsem.at[PE]).start()
+            pltpu.make_async_copy(esend.at[j, y2], erecv.at[z], rsem.at[PE]).start()
 
         @pl.when(jnp.logical_not(itself))
         def _():
-            send(PE, esend.at[x2, y2], erecv.at[t], (4 * y2 + x, b))
+            send(PE, esend.at[j, y2], erecv.at[z], (4 * y2 + x, b))
 
         return 0
 
-    lax.fori_loop(0, N, out_send, 0)
-    flights.append((PE, erecv.at[0:15]))
+    lax.fori_loop(0, 8, out_send, 0)
+    flights.append((PE, erecv.at[0:7]))
     over_ep(PMETA, lambda a: meta, metas.at[e_slot])
     flights.append((PMETA, metas.at[0:15]))
 
@@ -531,6 +558,11 @@
     for phase, blocks in flights:
         sent(phase, blocks)
 
+    @pl.when(other)
+    def _():
+        sent(PW1, wown)
+        sent(PW2, wo.at[0])
+
     if any(phase == PE for phase, _ in flights):
 
         @pl.when(t // 4 != y)
@@ -555,7 +587,8 @@
     scratch = [
         vmem((N, 4096), BF16),
         vmem((256, 512), BF16),
-        vmem((4, 256, 256), BF16),
+        vmem((256, 256), BF16),
+        vmem((2, 512, 256), BF16),
         vmem((1, 2), F32),
         vmem((1, 128), F32),
         vmem((CACHE, N * 128), BF16),
@@ -580,11 +613,11 @@
         vmem((N * 128, 128), BF16),
         vmem((CACHE, 128), F32),
         vmem((N, 256), BF16),
-        vmem((4, N, 256), BF16),
+        vmem((8, N, 256), BF16),
         vmem((2, 128), F32),
         vmem((N, 2, 128), F32),
-        vmem((4, 4, N, 256), BF16),
-        vmem((N, N, 256), BF16),
+        vmem((2, 4, N, 256), BF16),
+        vmem((8, N, 256), BF16),
         vmem((1, 128), F32),
         vmem((N, 1, 128), F32),
         vmem((2, 128), F32),

time: 75.2 us -> 73.4 us (0.976)
  Pallas kernels: 73.8 us -> 71.9 us
    pallas_call x1, Pallas kernels: 73.8 us -> 71.9 us  [on_device(): pl.pallas_call(kernel, out_shape=jax.ShapeDtypeStruct((N, 256), BF16), in...]
where the time goes in v4:
time: 73.4 us; the launch traced here: 73.2 us
  Pallas kernels  71.9 us (98%)
  local copies, waits for them, and re-layouts  1.3 us (2%)
    pallas_call x1, Pallas kernels, on_device(): pl.pallas_call(kernel, out_shape=jax.ShapeDtypeStruct((N, 256), BF16), in...  71.9 us

profile of v4, /device:TPU:1, one launch (start us, length us, event | category | flops | bytes accessed | tf_op | source)
XLA Modules:
  0.0 73.2 jit_solution(1782846762262300580)
XLA Ops:
  0.0 71.9 %layer.1 = bf16[16,256]{1,0:T(8,128)(2,1)} custom-call(bf16[16,4096]{1,0:T(8,128)(2,1)} %tok_h.1, bf16[256,256]{1,0:T(8,128)(2,1)} %qw_h.1, bf16[256,128]{1,0:T(8,128)(2,1)} %kw_h.1, bf16[256,128]{1,0:T(8,128)(2,1)} %vw_h.1, bf16[256,256]{1,0:T(8,128)(2,1)} %ow_h.1, f32[1,2]{1,0:T(1,128)} %bitcast.23, f32[1,128]{1,0:T(1,128)} %bitcast.24, ...), custom_call_target="tpu_custom_call" | custom-call | tf_op jit(solution)/shard_map/layer/pallas_call | solution.py:651
  71.9 1.3 %copy.23 = bf16[16,256]{1,0:T(8,128)(2,1)} copy(bf16[16,256]{1,0:T(8,128)(2,1)} %layer.1) | data formatting | bytes 16384

commit v5 on v4

--- a/solution.py
+++ b/solution.py
@@ -145,17 +145,18 @@
             device_id_type=MESH,
         ).start()
 
-    def over_ep(phase, src_of, dst):
-        def one(k, _):
-            a = lax.rem(e + k, N)
-            send(phase, src_of(a), dst, (a, t))
-            return 0
-
-        lax.fori_loop(1, N, one, 0)
-
     def far_first(i, n):
         half = (i + 1) // 2
         return n // 2 + half * (2 * lax.rem(i + 1, 2) - 1)
+
+    def over_ep(phase, src_of, dst):
+        def one(i, _):
+            dy, dx = far_first(i // 4, 4), far_first(lax.rem(i, 4), 4)
+            a = 4 * lax.rem(y + dy, 4) + lax.rem(x + dx, 4)
+            send(phase, src_of(a), dst, (a, t))
+            return 0
+
+        lax.fori_loop(0, N - 1, one, 0)
 
     def over_tp(phase, src_of, dst):
         def one(i, _):
@@ -260,6 +261,7 @@
     over_ep(PV, lambda a: vsend, vrecv.at[e])
     flights.append((PV, vrecv.at[0:15]))
 
+    received(PB, brecv.at[0:15])
     arrived("eg")
     arrived("eu")
     arrived("dg")
@@ -269,7 +271,6 @@
     send(PWD, wd, wd2, partner)
     flights.append((PWD, wd2))
 
-    received(PB, brecv.at[0:15])
     qkv = jnp.sum(brecv[...].astype(F32), axis=0).astype(BF16).astype(F32)
 
     def rotated(v):

time: 73.4 us -> 72.7 us (level)
  no operation moved by 1% of the time
where the time goes in v5:
time: 72.7 us; the launch traced here: 72.6 us
  Pallas kernels  71.3 us (98%)
  local copies, waits for them, and re-layouts  1.3 us (2%)
    pallas_call x1, Pallas kernels, on_device(): pl.pallas_call(kernel, out_shape=jax.ShapeDtypeStruct((N, 256), BF16), in...  71.3 us

profile of v5, /device:TPU:1, one launch (start us, length us, event | category | flops | bytes accessed | tf_op | source)
XLA Modules:
  0.0 72.6 jit_solution(4985095692209786308)
XLA Ops:
  0.0 71.3 %layer.1 = bf16[16,256]{1,0:T(8,128)(2,1)} custom-call(bf16[16,4096]{1,0:T(8,128)(2,1)} %tok_h.1, bf16[256,256]{1,0:T(8,128)(2,1)} %qw_h.1, bf16[256,128]{1,0:T(8,128)(2,1)} %kw_h.1, bf16[256,128]{1,0:T(8,128)(2,1)} %vw_h.1, bf16[256,256]{1,0:T(8,128)(2,1)} %ow_h.1, f32[1,2]{1,0:T(1,128)} %bitcast.23, f32[1,128]{1,0:T(1,128)} %bitcast.24, ...), custom_call_target="tpu_custom_call" | custom-call | tf_op jit(solution)/shard_map/layer/pallas_call | solution.py:652
  71.3 1.3 %copy.23 = bf16[16,256]{1,0:T(8,128)(2,1)} copy(bf16[16,256]{1,0:T(8,128)(2,1)} %layer.1) | data formatting | bytes 16384
